TPU v7x, 512 devices: a whole 4x4x16 slice. The times are simulated.
512 devices in a mesh: sp: 32 (over z, core), tp: 16 (over y, x).
Axes of the slice: x: 4, y: 4, z: 16, core: 2. Of those that a mesh axis runs over, the one named last changes fastest.
Arguments:
- moe_input: bfloat16 [10240, 2048], P('sp', 'tp'), may hold values from -6 to 6
- out_cotangent: bfloat16 [10240, 2048], P('sp', 'tp'), may hold values from -0.59765625 to 0.59765625
- routes: int32 [10240, 2], P('sp'), may hold values from 0 to 31, all different within a row; in each aligned block of 320 rows (0 to 319, 320 to 639, ...) at most 30 rows name the same one
- route_weight: float32 [10240, 2], P('sp'), may hold values from 0.1 to 0.9
- gate_weight: bfloat16 [32, 1024, 2048], P('sp', 'tp'), may hold values from -0.125 to 0.125
- up_weight: bfloat16 [32, 1024, 2048], P('sp', 'tp'), may hold values from -0.125 to 0.125
- down_weight: bfloat16 [32, 1024, 2048], P('sp', 'tp'), may hold values from -0.1875 to 0.1875
- glu_value: bfloat16 [10240, 1024], P('sp', 'tp'), may hold values from -6 to 6
- glu_gate: bfloat16 [10240, 1024], P('sp', 'tp'), may hold values from -8 to 8
- conv_result: bfloat16 [10240, 1024], P('sp', 'tp'), may hold values from -12 to 12
- conv_taps: float32 [31, 1024], P(None, 'tp'), may hold values from -1 to 1
- norm_gain: float32 [1024], P('tp'), may hold values from 0.1 to 1.9
- proj_weight: bfloat16 [1024, 2048], P('tp'), may hold values from -0.1875 to 0.1875
Outputs:
- grad_gate: float32 [32, 1024, 2048], P('sp', 'tp')
- grad_up: float32 [32, 1024, 2048], P('sp', 'tp')
- grad_down: float32 [32, 1024, 2048], P('sp', 'tp')
- grad_proj: float32 [2048, 1024], P('sp', 'tp')
- grad_value: bfloat16 [10240, 1024], P('sp', 'tp')
- grad_glu_gate: bfloat16 [10240, 1024], P('sp', 'tp')
Inputs may be any that keep to these rules, and one draw needn't show every extreme that they name: `routes`: each row names two different experts. In the aligned blocks of 320 rows (the rows of one index of sp) no expert is named by more than 30 rows, and that bound is reached.
All inputs are finite; a program needn't handle non-finite values.
Results may differ from a plain program's by a relative error of at most 0.025.
Values may be sent and summed in bfloat16 or wider, within the bound.
No kernel may reach another device: no remote copies, remote signals or barrier semaphores. Data moves between devices by JAX's collectives and lax.ppermute only.
A program may use at most 64 MiB of HBM per device.

v0:
```python
import jax
import jax.numpy as jnp
import numpy as np
from jax import lax
from jax.experimental import pallas as pl
from jax.experimental.pallas import tpu as pltpu
from jax.sharding import Mesh
from jax.sharding import PartitionSpec as P

NORM_EPS = 0.25
SP = ("z", "c")
TP = ("y", "x")
PLANE = ("c", "y", "x")
SIDE = 4
SLOT = 32
ROOM = 12 << 20
BF = jnp.bfloat16
F32 = jnp.float32
VM = pltpu.VMEM

NT = (((1,), (1,)), ((), ()))
TN = (((0,), (0,)), ((), ()))
NN = (((1,), (0,)), ((), ()))


def place(core, row, col):
    return core * SIDE * SIDE + row * SIDE + col


def plane_groups():
    r = range(SIDE)
    down = [[[place(k, y, x) for y in r] for x in r] for k in (0, 1)]
    across = [[[place(k, y, x) for x in r] for y in r] for k in (0, 1)]
    return down[0] + across[1], across[0] + down[1]


def step_tables():
    features, units = plane_groups()
    of_features = {p: g for g in features for p in g}
    table = np.zeros((2 * SIDE * SIDE, 64), np.int32)
    for group in units:
        for me, p in enumerate(group):
            table[p, 0] = me
            table[p, 1] = of_features[p].index(p)
            table[p, 2] = p // (SIDE * SIDE)
            for k in range(SIDE):
                ahead = of_features[group[(me + k) % SIDE]]
                back = of_features[group[(me - k) % SIDE]]
                for a in range(SIDE):
                    table[p, 16 + k * SIDE + a] = ahead[a] % (SIDE * SIDE)
                    table[p, 32 + k * SIDE + a] = back[a] % (SIDE * SIDE)
    of_units = {p: g for g in units for p in g}
    for p in range(2 * SIDE * SIDE):
        group = of_features[p]
        for j in range(SIDE):
            source = group[(group.index(p) - j) % SIDE]
            their = of_units[source]
            for k in range(SIDE):
                first = their[(their.index(source) - k) % SIDE]
                table[p, 48 + j * SIDE + k] = first % (SIDE * SIDE)
    return table


def steps_ahead(groups, k):
    return [(g[i], g[(i + k) % SIDE]) for g in groups for i in range(SIDE)]


def shift(part, groups, k):
    return lax.ppermute(part, PLANE, steps_ahead(groups, k))


def pass_on(parts, groups):
    return (parts[0],) + tuple(shift(parts[k], groups, k) for k in range(1, SIDE))


def mm(a, b, dims):
    return lax.dot_general(a, b, dims, preferred_element_type=F32)


def exchange(v, groups):
    return lax.all_to_all(v, PLANE, 0, 0, axis_index_groups=groups, tiled=True)


def cost(flops, nbytes):
    return pl.CostEstimate(flops=flops, bytes_accessed=nbytes, transcendentals=0)


def route_kernel(rt_ref, w_ref, x_ref, c_ref, s_ref, t_ref):
    tokens = rt_ref.shape[1]
    experts = s_ref.shape[0] // SLOT
    first, second = rt_ref[0:1, :], rt_ref[1:2, :]
    ids = lax.broadcasted_iota(jnp.int32, (experts, tokens), 0)
    o0, o1 = ids == first, ids == second
    both = jnp.where(o0 | o1, 1.0, 0.0).astype(BF)
    before = lax.broadcasted_iota(jnp.int32, (tokens, tokens), 0) < lax.broadcasted_iota(
        jnp.int32, (tokens, tokens), 1
    )
    earlier = mm(both, jnp.where(before, 1.0, 0.0).astype(BF), NN)
    rank0 = jnp.sum(jnp.where(o0, earlier, 0.0), axis=0, keepdims=True)
    rank1 = jnp.sum(jnp.where(o1, earlier, 0.0), axis=0, keepdims=True)
    t0 = first * SLOT + rank0.astype(jnp.int32)
    t1 = second * SLOT + rank1.astype(jnp.int32)
    t_ref[0:1, :] = t0
    t_ref[1:2, :] = t1
    w0, w1 = w_ref[0:1, :], w_ref[1:2, :]
    x, c = x_ref[...], c_ref[...]
    size = 128
    for k in range(s_ref.shape[0] // size):
        slots = lax.broadcasted_iota(jnp.int32, (size, tokens), 0) + k * size
        m0, m1 = slots == t0, slots == t1
        pick = jnp.where(m0 | m1, 1.0, 0.0).astype(BF)
        weight = jnp.sum(
            jnp.where(m0, w0, 0.0) + jnp.where(m1, w1, 0.0), axis=1, keepdims=True
        )
        rows = pl.ds(k * size, size)
        s_ref[rows, 0:128] = mm(pick, x, NN).astype(BF)
        s_ref[rows, 128:256] = (weight * mm(pick, c, NN)).astype(BF)


def pick_kernel(t_ref, p_ref):
    slots = lax.broadcasted_iota(jnp.int32, p_ref.shape, 0)
    held = (slots == t_ref[0:1, :]) | (slots == t_ref[1:2, :])
    p_ref[...] = jnp.where(held, 1.0, 0.0).astype(BF)


def split_kernel(at_ref, g_ref, u_ref, d_ref, p_ref, c_ref, *outs):
    for k, out in enumerate(outs):
        for a in range(SIDE):
            at = at_ref[16 + k * SIDE + a]
            cols = pl.ds(pl.multiple_of(at * 128, 128), 128)
            for q, ref in enumerate((g_ref, u_ref, d_ref, p_ref)):
                out[q * 64 : q * 64 + 64, a * 128 : a * 128 + 128] = ref[:, cols]
        out[256:320, :] = c_ref[...]


def relay_kernel(at_ref, r0, r1, r2, r3, *outs):
    for j, out in enumerate(outs):
        a = lax.rem(at_ref[1] + j, SIDE)
        cols = pl.ds(pl.multiple_of(a * 128, 128), 128)
        for k, r_ref in enumerate((r0, r1, r2, r3)):
            out[k * 64 : k * 64 + 64, 0:128] = r_ref[192:256, cols]
            out[k * 64 : k * 64 + 64, 128:512] = r_ref[256:320, 128:512]


def merge_kernel(at_ref, s0, s1, s2, s3, g_ref, u_ref, d_ref):
    for k, s_ref in enumerate((s0, s1, s2, s3)):
        for a in range(SIDE):
            at = at_ref[32 + k * SIDE + a]
            cols = pl.ds(pl.multiple_of(at * 128, 128), 128)
            for q, ref in enumerate((g_ref, u_ref, d_ref)):
                ref[:, cols] = s_ref[
                    q * 64 : q * 64 + 64, a * 128 : a * 128 + 128
                ].astype(F32)


def behind_of(at_ref, k):
    return lax.rem(at_ref[0] + (SIDE - k), SIDE)


def ahead_of(at_ref, k):
    return lax.rem(at_ref[0] + k, SIDE)


def pre_kernel(at_ref, a_ref, w0, w1, w2, w3, o_ref):
    ws = (w0, w1, w2, w3)
    x = jnp.concatenate([a_ref[i, :, 0:128] for i in range(SIDE)], axis=1)
    c = jnp.concatenate([a_ref[i, :, 128:256] for i in range(SIDE)], axis=1)
    pairs = mm(jnp.concatenate([w[0:128, :] for w in ws], axis=0), x, NT)
    downs = mm(jnp.concatenate([w[128:192, :] for w in ws], axis=0), c, NT)
    for k in range(SIDE):
        b = behind_of(at_ref, k)
        o_ref[b, 0:128, :] = pairs[k * 128 : k * 128 + 128].astype(BF)
        o_ref[b, 128:192, :] = downs[k * 64 : k * 64 + 64].astype(BF)


def gate_kernel(p_ref, o_ref):
    total = p_ref[0].astype(F32)
    for b in range(1, SIDE):
        total = total + p_ref[b].astype(F32)
    gate, up, cot = total[0:64], total[64:128], total[128:192]
    s = jax.nn.sigmoid(gate)
    act = gate * s
    hidden = (act * up).astype(BF)
    up_cot = (cot * act).astype(BF)
    gate_cot = (cot * up * s * (1.0 + gate * (1.0 - s))).astype(BF)
    for b in range(SIDE):
        o_ref[b, 0:64, :] = gate_cot
        o_ref[b, 64:128, :] = up_cot
        o_ref[b, 128:192, :] = hidden


def partial_kernel(at_ref, h_ref, w0, w1, w2, w3, o_ref):
    ws = (w0, w1, w2, w3)
    h = jnp.concatenate([h_ref[behind_of(at_ref, k), 0:128, :] for k in range(SIDE)], axis=0)
    w = jnp.concatenate([w_ref[0:128, :] for w_ref in ws], axis=0)
    total = mm(h, w, TN)
    for a in range(SIDE):
        o_ref[a] = total[:, a * 128 : a * 128 + 128].astype(BF)


def grads_kernel(at_ref, h_ref, a_ref, *outs):
    x = jnp.concatenate([a_ref[0, :, 0:128], a_ref[1, :, 0:128]], axis=1)
    c = jnp.concatenate([a_ref[0, :, 128:256], a_ref[1, :, 128:256]], axis=1)
    order = [ahead_of(at_ref, k) for k in range(SIDE)]
    pairs = mm(jnp.concatenate([h_ref[b, 0:128, :] for b in order], axis=0), x, NN)
    downs = mm(jnp.concatenate([h_ref[b, 128:192, :] for b in order], axis=0), c, NN)
    for k, out in enumerate(outs):
        out[0:128, :] = pairs[k * 128 : k * 128 + 128].astype(BF)
        out[128:192, :] = downs[k * 64 : k * 64 + 64].astype(BF)


def total_kernel(
    at_ref, p_ref, r_ref, c_ref, q0, q1, q2, q3, mine_ref, other_ref, total_ref, stats_ref
):
    qs = (q0, q1, q2, q3)
    moe = mm(p_ref[...], r_ref[...], TN)
    total = (c_ref[...].astype(F32) + moe).astype(BF)
    tokens = total.shape[0]
    total_ref[0:tokens, :] = total
    total_ref[tokens:, :] = jnp.zeros((total_ref.shape[0] - tokens, 128), BF)
    size = q0.shape[0]
    channels = SIDE * size
    mean = jnp.zeros((1, tokens), F32)
    for q in qs:
        conv = q[:, 128 : 128 + tokens].astype(F32)
        mean = mean + jnp.sum(conv, axis=0, keepdims=True)
    mean = mean / channels
    var = jnp.zeros((1, tokens), F32)
    for q in qs:
        off = q[:, 128 : 128 + tokens].astype(F32) - mean
        var = var + jnp.sum(off * off, axis=0, keepdims=True)
    inv = lax.rsqrt(var / channels + NORM_EPS)
    stats_ref[0:1, :] = mean
    stats_ref[1:2, :] = inv
    own = jnp.full((64, 128), at_ref[2], jnp.int32) == 0
    for j, q in enumerate(qs):
        normed = (q[:, 128 : 128 + tokens].astype(F32) - mean) * inv
        linear = normed * gain_of(q)
        act = (linear * jax.nn.sigmoid(linear)).astype(BF)
        grad = mm(act, total, NN)
        turned = pltpu.roll(grad, 64, 1)
        for k in range(SIDE):
            b = at_ref[48 + j * SIDE + k]
            rows = slice(k * 64, k * 64 + 64)
            mine_ref[b] = jnp.where(own, turned[rows], grad[rows]).astype(BF)
            other_ref[b] = jnp.where(own, grad[rows], turned[rows]).astype(BF)


def gain_of(q):
    lane = lax.broadcasted_iota(jnp.int32, (q.shape[0], 128), 1)
    pieces = jnp.where((lane >= 64) & (lane < 67), q[:, 384:512].astype(F32), 0.0)
    return jnp.sum(pieces, axis=1, keepdims=True)


def cot_kernel(at_ref, total_ref, stats_ref, q0, q1, q2, q3, o_ref):
    wide = total_ref.shape[0]
    tokens = stats_ref.shape[1]
    total = total_ref[...]
    mean, inv = stats_ref[0:1, :], stats_ref[1:2, :]
    first = jnp.zeros((1, tokens), F32)
    second = jnp.zeros((1, tokens), F32)
    for j, q in enumerate((q0, q1, q2, q3)):
        normed = (q[:, 128 : 128 + tokens].astype(F32) - mean) * inv
        gain = gain_of(q)
        linear = normed * gain
        s = jax.nn.sigmoid(linear)
        cot = mm(q[:, 0:128], total, NT)
        sloped = cot[:, 0:tokens] * (s * (1.0 + linear * (1.0 - s)) * gain)
        first = first + jnp.sum(sloped, axis=0, keepdims=True)
        second = second + jnp.sum(sloped * normed, axis=0, keepdims=True)
        for k in range(SIDE):
            o_ref[at_ref[48 + j * SIDE + k], 0:64, :] = cot[k * 64 : k * 64 + 64].astype(BF)
    row = lax.broadcasted_iota(jnp.int32, (8, tokens), 0)
    sums = jnp.zeros((8, tokens), F32)
    for i, v in enumerate((first, second)):
        head = v.astype(BF).astype(F32)
        sums = jnp.where(row == 2 * i, head, jnp.where(row == 2 * i + 1, v - head, sums))
    for b in range(o_ref.shape[0]):
        o_ref[b, 64:72, 0:tokens] = sums.astype(BF)
        o_ref[b, 64:72, tokens:wide] = jnp.zeros((8, wide - tokens), BF)


def join_kernel(a_ref, mine_ref, other_ref, o_ref):
    low = lax.broadcasted_iota(jnp.int32, (64, 128), 1) < 64
    for b in range(o_ref.shape[0]):
        piece = mine_ref[b].astype(F32) + other_ref[b].astype(F32)
        o_ref[b, 0:64, :] = jnp.where(low, a_ref[b, 0:64, :].astype(F32), piece).astype(BF)
        o_ref[b, 64:72, :] = a_ref[b, 64:72, :]


def part_kernel(r_ref, o_ref):
    low = lax.broadcasted_iota(jnp.int32, (32, 128), 1) < 64
    for b in range(o_ref.shape[0]):
        upper = pltpu.roll(r_ref[b, 0:32, 256:384].astype(F32), 64, 1)
        lower = r_ref[b, 32:64, 256:384].astype(F32)
        o_ref[b] = jnp.where(low, upper, lower).astype(BF)


def head_kernel(r_ref, conv_ref, stats_ref, gain_ref, o_ref, h_ref):
    tokens = conv_ref.shape[1]
    total = r_ref[0, :, 0:tokens].astype(F32)
    for b in range(1, r_ref.shape[0]):
        total = total + r_ref[b, :, 0:tokens].astype(F32)
    channels = 16 * conv_ref.shape[0]
    first = (total[64:65] + total[65:66]) / channels
    second = (total[66:67] + total[67:68]) / channels
    inv = stats_ref[1:2, :]
    normed = (conv_ref[...].astype(F32) - stats_ref[0:1, :]) * inv
    gain = gain_ref[...]
    linear = normed * gain
    s = jax.nn.sigmoid(linear)
    cot = total[0:64] * s * (1.0 + linear * (1.0 - s)) * gain
    cot = inv * (cot - first - normed * second)
    o_ref[...] = cot
    h_ref[...] = cot[:, 0:128]


def sum_kernel(a_ref, o_ref):
    total = a_ref[0].astype(F32)
    for b in range(1, a_ref.shape[0]):
        total = total + a_ref[b].astype(F32)
    turned = pltpu.roll(total, 64, 1)
    block = jnp.concatenate([total, turned], axis=0)
    o_ref[...] = block.T[0:64, :]


def sum_side_kernel(p_ref, o_ref):
    total = p_ref[0].astype(F32)
    for a in range(1, SIDE):
        total = total + p_ref[a].astype(F32)
    o_ref[...] = total.astype(BF)


def conv_kernel(cot_ref, next_ref, taps_ref, gate_ref, value_ref, v_ref, g_ref, buf):
    rows, tokens = cot_ref.shape
    wide = buf.shape[1]
    reach = taps_ref.shape[1] - 1
    buf[:, 0:128] = next_ref[...]
    buf[:, 128:wide] = jnp.zeros((rows, wide - 128), F32)
    after = pltpu.roll(buf[...], tokens, 1)
    buf[:, 0:tokens] = cot_ref[...]
    lane = lax.broadcasted_iota(jnp.int32, (rows, wide), 1)
    whole = jnp.where(lane < tokens, buf[...], after)
    taps = taps_ref[...]
    total = whole * taps[:, reach : reach + 1]
    for s in range(1, reach + 1):
        total = total + pltpu.roll(whole, wide - s, 1) * taps[:, reach - s : reach - s + 1]
    cot = total[:, 0:tokens]
    s = jax.nn.sigmoid(gate_ref[...].astype(F32))
    v_ref[...] = (cot * s).astype(BF)
    g_ref[...] = (cot * value_ref[...].astype(F32) * s * (1.0 - s)).astype(BF)


def whole(shape, dtype):
    return jax.ShapeDtypeStruct(shape, dtype)


def body(
    moe_input,
    out_cotangent,
    routes,
    route_weight,
    gate_weight,
    up_weight,
    down_weight,
    glu_value,
    glu_gate,
    conv_result,
    conv_taps,
    norm_gain,
    proj_weight,
):
    sp_count = lax.axis_size(SP)
    tp_count = lax.axis_size(TP)
    tokens = moe_input.shape[0]
    slots = sp_count * SLOT
    feature_groups, unit_groups = plane_groups()
    smem = pl.BlockSpec(memory_space=pltpu.SMEM)
    vmem = pl.BlockSpec(memory_space=VM)
    room = pltpu.CompilerParams(vmem_limit_bytes=ROOM)

    sent, target = pl.pallas_call(
        route_kernel,
        out_shape=(whole((slots, 256), BF), whole((2, tokens), jnp.int32)),
        in_specs=[vmem] * 4,
        out_specs=(vmem, vmem),
        cost_estimate=cost(400000000, 2000000),
        name="route",
    )(routes.T, route_weight.T, moe_input, out_cotangent)
    sent, target, table, gate_weight, conv_result, norm_gain = lax.optimization_barrier(
        (sent, target, jnp.asarray(step_tables()), gate_weight, conv_result, norm_gain)
    )
    at = table[lax.axis_index(PLANE)]
    pick = pl.pallas_call(
        pick_kernel,
        out_shape=whole((slots, tokens), BF),
        in_specs=[vmem],
        out_specs=vmem,
        compiler_params=room,
        cost_estimate=cost(1000000, 700000),
        name="pick",
    )(target)
    conv_t = conv_result.T
    gain = norm_gain.reshape(-1, 1)
    high = lax.reduce_precision(gain, 8, 7)
    middle = lax.reduce_precision(gain - high, 8, 7)
    pieces = jnp.concatenate([high, middle, gain - high - middle], axis=1).astype(BF)
    channel_part = jnp.concatenate(
        [jnp.zeros((64, 128), BF), conv_t, pieces, jnp.zeros((64, 61), BF)], axis=1
    )
    split = pl.pallas_call(
        split_kernel,
        out_shape=(whole((320, 512), BF),) * SIDE,
        in_specs=[smem] + [vmem] * 5,
        out_specs=(vmem,) * SIDE,
        compiler_params=room,
        cost_estimate=cost(1000000, 2600000),
        name="split_weights",
    )(at, gate_weight[0], up_weight[0], down_weight[0], proj_weight, channel_part)
    weights = pass_on(split, unit_groups)
    relay = pl.pallas_call(
        relay_kernel,
        out_shape=(whole((256, 512), BF),) * SIDE,
        in_specs=[smem] + [vmem] * SIDE,
        out_specs=(vmem,) * SIDE,
        compiler_params=room,
        cost_estimate=cost(1000000, 2000000),
        name="relay",
    )(at, *weights)
    arrived = shift(relay[1], feature_groups, 1)
    got = lax.all_to_all(sent.reshape(sp_count, SLOT, 256), SP, 0, 0, tiled=True)
    got = got.reshape(slots, 256)
    got, weights, relay, arrived = lax.optimization_barrier((got, weights, relay, arrived))
    taps_t = conv_taps.T

    rows = exchange(jnp.broadcast_to(got[None], (SIDE, slots, 256)), feature_groups)
    step = 256
    pre = pl.pallas_call(
        pre_kernel,
        grid=(slots // step,),
        out_shape=whole((SIDE, 192, slots), BF),
        in_specs=[smem, pl.BlockSpec((SIDE, step, 256), lambda i: (0, i, 0))]
        + [pl.BlockSpec((192, 512), lambda i: (0, 0))] * SIDE,
        out_specs=pl.BlockSpec((SIDE, 192, step), lambda i: (0, 0, i)),
        compiler_params=room,
        cost_estimate=cost(800000000, 4400000),
        name="pre",
    )(at, rows, *weights)
    pre = exchange(pre, unit_groups)
    hidden = pl.pallas_call(
        gate_kernel,
        grid=(slots // step,),
        out_shape=whole((SIDE, 192, slots), BF),
        in_specs=[pl.BlockSpec((SIDE, 192, step), lambda i: (0, 0, i))],
        out_specs=pl.BlockSpec((SIDE, 192, step), lambda i: (0, 0, i)),
        compiler_params=room,
        cost_estimate=cost(3000000, 3200000),
        name="gates",
    )(pre)
    hidden = exchange(hidden, unit_groups)
    part = pl.pallas_call(
        partial_kernel,
        grid=(slots // step,),
        out_shape=whole((SIDE, slots, 128), BF),
        in_specs=[smem, pl.BlockSpec((SIDE, 192, step), lambda i: (0, 0, i))]
        + [pl.BlockSpec((192, 512), lambda i: (0, 0))] * SIDE,
        out_specs=pl.BlockSpec((SIDE, step, 128), lambda i: (0, i, 0)),
        compiler_params=room,
        cost_estimate=cost(540000000, 3400000),
        name="partial",
    )(at, hidden, *weights)
    part = exchange(part, feature_groups)
    back = pl.pallas_call(
        sum_side_kernel,
        out_shape=whole((slots, 128), BF),
        in_specs=[vmem],
        out_specs=vmem,
        compiler_params=room,
        cost_estimate=cost(1000000, 1300000),
        name="sum_side",
    )(part).reshape(sp_count, SLOT, 128)
    back, relay = lax.optimization_barrier((back, relay))
    relay = (relay[0], arrived, shift(relay[2], feature_groups, 2), shift(relay[3], feature_groups, 3))
    returned = lax.all_to_all(back, SP, 0, 0, tiled=True).reshape(slots, 128)

    grads = pl.pallas_call(
        grads_kernel,
        grid=(SIDE // 2,),
        out_shape=(whole((192, 512), BF),) * SIDE,
        in_specs=[
            smem,
            pl.BlockSpec((SIDE, 192, slots), lambda i: (0, 0, 0)),
            pl.BlockSpec((2, slots, 256), lambda i: (i, 0, 0)),
        ],
        out_specs=(pl.BlockSpec((192, 256), lambda i: (0, i)),) * SIDE,
        compiler_params=room,
        cost_estimate=cost(800000000, 4400000),
        name="grads",
    )(at, hidden, rows)
    first_grad = shift(grads[1], unit_groups, 1)
    returned, grads, first_grad = lax.optimization_barrier((returned, grads, first_grad))

    wide = 384
    mine, other, total_cot, stats = pl.pallas_call(
        total_kernel,
        out_shape=(
            whole((tp_count, 64, 128), BF),
            whole((tp_count, 64, 128), BF),
            whole((wide, 128), BF),
            whole((2, tokens), F32),
        ),
        in_specs=[smem] + [vmem] * 7,
        out_specs=(vmem,) * 4,
        compiler_params=room,
        cost_estimate=cost(170000000, 2500000),
        name="total_cot",
    )(at, pick, returned, out_cotangent, *relay)
    other = lax.ppermute(other, "c", [(0, 1), (1, 0)])
    act_part = pl.pallas_call(
        cot_kernel,
        out_shape=whole((tp_count, 72, wide), BF),
        in_specs=[smem] + [vmem] * 6,
        out_specs=vmem,
        compiler_params=room,
        cost_estimate=cost(100000000, 2500000),
        name="act_cot",
    )(at, total_cot, stats, *relay)
    act_part = pl.pallas_call(
        join_kernel,
        grid=(1,),
        out_shape=whole((tp_count, 72, wide), BF),
        in_specs=[
            pl.BlockSpec((tp_count, 72, 128), lambda i: (0, 0, 2)),
            pl.BlockSpec((tp_count, 64, 128), lambda i: (0, 0, 0)),
            pl.BlockSpec((tp_count, 64, 128), lambda i: (0, 0, 0)),
        ],
        out_specs=pl.BlockSpec((tp_count, 72, 128), lambda i: (0, 0, 2)),
        input_output_aliases={0: 0},
        compiler_params=room,
        cost_estimate=cost(100000, 1200000),
        name="join_cores",
    )(act_part, mine, other)
    act_part = lax.all_to_all(act_part, TP, 0, 0, tiled=True)
    proj_part = pl.pallas_call(
        part_kernel,
        out_shape=whole((tp_count, 32, 128), BF),
        in_specs=[vmem],
        out_specs=vmem,
        compiler_params=room,
        cost_estimate=cost(100000, 400000),
        name="proj_part",
    )(act_part)
    act_part, proj_part, grads = lax.optimization_barrier((act_part, proj_part, grads))
    grads = (grads[0], first_grad, shift(grads[2], unit_groups, 2), shift(grads[3], unit_groups, 3))
    proj_part = lax.all_to_all(proj_part, "z", 0, 0, tiled=True)
    grad_proj = pl.pallas_call(
        sum_kernel,
        out_shape=whole((64, 64), F32),
        in_specs=[vmem],
        out_specs=vmem,
        compiler_params=room,
        cost_estimate=cost(100000, 200000),
        name="sum_planes",
    )(proj_part)

    conv_cot, head = pl.pallas_call(
        head_kernel,
        out_shape=(whole((64, tokens), F32), whole((64, 128), F32)),
        in_specs=[vmem] * 4,
        out_specs=(vmem, vmem),
        compiler_params=room,
        cost_estimate=cost(3000000, 1200000),
        name="conv_cot",
    )(act_part, conv_t, stats, gain)
    behind = [(i + 1, i) for i in range(sp_count - 1)]
    after = lax.ppermute(head, SP, behind)
    value, gate = pl.pallas_call(
        conv_kernel,
        out_shape=(whole((64, tokens), BF), whole((64, tokens), BF)),
        in_specs=[vmem] * 5,
        out_specs=(vmem, vmem),
        scratch_shapes=[VM((64, 384), F32)],
        compiler_params=room,
        cost_estimate=cost(4000000, 400000),
        name="conv",
    )(conv_cot, after, taps_t, glu_gate.T, glu_value.T)

    grad_gate, grad_up, grad_down = pl.pallas_call(
        merge_kernel,
        out_shape=(whole((64, 2048), F32),) * 3,
        in_specs=[smem] + [vmem] * SIDE,
        out_specs=(vmem,) * 3,
        compiler_params=room,
        cost_estimate=cost(1000000, 2400000),
        name="merge_grads",
    )(at, *grads)
    return (
        grad_gate[None],
        grad_up[None],
        grad_down[None],
        grad_proj,
        value.T,
        gate.T,
    )


def solution(mesh):
    split = Mesh(mesh.devices.reshape(16, 2, SIDE, SIDE), ("z", "c", "y", "x"))
    placed = (
        P(SP, TP),
        P(SP, TP),
        P(SP, None),
        P(SP, None),
        P(SP, TP, None),
        P(SP, TP, None),
        P(SP, TP, None),
        P(SP, TP),
        P(SP, TP),
        P(SP, TP),
        P(None, TP),
        P(TP),
        P(TP, None),
    )
    return jax.shard_map(
        body,
        mesh=split,
        in_specs=placed,
        out_specs=(
            P(SP, TP, None),
            P(SP, TP, None),
            P(SP, TP, None),
            P(SP, TP),
            P(SP, TP),
            P(SP, TP),
        ),
        check_vma=False,
    )
```

profile of v0, /device:TPU:1, one launch (start us, length us, event | category | flops | bytes accessed | tf_op | source)
XLA Modules:
  0.0 212.7 jit_solution(15827031380002246054)
XLA Ops:
  0.7 2.9 %route.1 = (bf16[1024,256]{1,0:T(8,128)(2,1)}, s32[2,320]{1,0:T(2,128)}) custom-call(s32[2,320]{1,0:T(2,128)} %bitcast.43, f32[2,320]{1,0:T(2,128)} %bitcast.44, bf16[320,128]{1,0:T(8,128)(2,1)} %x_ref.1, bf16[320,128]{1,0:T(8,128)(2,1)} %c_ref.3), custom_call_target="tpu_custom_call" | custom-call | flops 400000000 | bytes 2000000 | tf_op jit(solution)/shard_map/route/pallas_call | solution.py:382
  3.6 16.8 %all-to-all-start = ((bf16[32,32,256]{2,1,0:T(8,128)(2,1)}), bf16[32,32,256]{2,1,0:T(8,128)(2,1)}, u32[]{:S(2)}, u32[]{:S(2)}) async-start(bf16[32,32,256]{2,1,0:T(8,128)(2,1)} %bitcast.36), calls=%async_computation | async-start | bytes 1048576 | tf_op jit(solution)/shard_map/all_to_all | solution.py:431
  22.5 3.2 %collective-permute-start = (bf16[320,512]{1,0:T(8,128)(2,1)S(1)}, bf16[320,512]{1,0:T(8,128)(2,1)S(1)}, u32[]{:S(2)}, u32[]{:S(2)}) collective-permute-start(bf16[320,512]{1,0:T(8,128)(2,1)S(1)} %get-tuple-element.69), channel_id=1, source_target_pairs={{0,1},{1,2},{2,3},{3,0},{4,5},{5,6},{6,7},{7,4},{8,9},{9,10},{10,1... | collective-permute-start | bytes 983048 | tf_op jit(solution)/shard_map/ppermute | solution.py:69
  25.7 4.5 %collective-permute-start.1 = (bf16[320,512]{1,0:T(8,128)(2,1)S(1)}, bf16[320,512]{1,0:T(8,128)(2,1)S(1)}, u32[]{:S(2)}, u32[]{:S(2)}) collective-permute-start(bf16[320,512]{1,0:T(8,128)(2,1)S(1)} %get-tuple-element.70), channel_id=1, source_target_pairs={{0,2},{1,3},{2,0},{3,1},{4,6},{5,7},{6,4},{7,5},{8,10},{9,11},{10,... | collective-permute-start | bytes 983048 | tf_op jit(solution)/shard_map/ppermute | solution.py:69
  30.2 3.0 %collective-permute-start.2 = (bf16[320,512]{1,0:T(8,128)(2,1)S(1)}, bf16[320,512]{1,0:T(8,128)(2,1)S(1)}, u32[]{:S(2)}, u32[]{:S(2)}) collective-permute-start(bf16[320,512]{1,0:T(8,128)(2,1)S(1)} %get-tuple-element.71), channel_id=1, source_target_pairs={{0,3},{1,0},{2,1},{3,2},{4,7},{5,4},{6,5},{7,6},{8,11},{9,8},{10,9... | collective-permute-start | bytes 983048 | tf_op jit(solution)/shard_map/ppermute | solution.py:69
  33.2 3.3 %collective-permute-done.1.r2.w2 = bf16[320,512]{1,0:T(8,128)(2,1)S(1)} collective-permute-done((bf16[320,512]{1,0:T(8,128)(2,1)S(1)}, bf16[320,512]{1,0:T(8,128)(2,1)S(1)}, u32[]{:S(2)}, u32[]{:S(2)}) %collective-permute-start.1) | collective-permute-done | bytes 327712 | tf_op jit(solution)/shard_map/ppermute | solution.py:69
  41.2 3.1 %collective-permute-start.3 = (bf16[256,512]{1,0:T(8,128)(2,1)S(1)}, bf16[256,512]{1,0:T(8,128)(2,1)S(1)}, u32[]{:S(2)}, u32[]{:S(2)}) collective-permute-start(bf16[256,512]{1,0:T(8,128)(2,1)S(1)} %get-tuple-element.73), channel_id=1, source_target_pairs={{0,4},{4,8},{8,12},{12,0},{1,5},{5,9},{9,13},{13,1},{2,6},{6,10},{... | collective-permute-start | bytes 786440 | tf_op jit(solution)/shard_map/ppermute | solution.py:69
  44.3 5.5 %collective-permute-done.3.q1 = bf16[256,512]{1,0:T(8,128)(2,1)S(1)} collective-permute-done((bf16[256,512]{1,0:T(8,128)(2,1)S(1)}, bf16[256,512]{1,0:T(8,128)(2,1)S(1)}, u32[]{:S(2)}, u32[]{:S(2)}) %collective-permute-start.3) | collective-permute-done | bytes 262176 | tf_op jit(solution)/shard_map/ppermute | solution.py:69
  50.5 3.4 %all-to-all-done = bf16[32,32,256]{2,1,0:T(8,128)(2,1)} async-done(((bf16[32,32,256]{2,1,0:T(8,128)(2,1)}), bf16[32,32,256]{2,1,0:T(8,128)(2,1)}, u32[]{:S(2)}, u32[]{:S(2)}) %all-to-all-start) | async-done | bytes 524320 | tf_op jit(solution)/shard_map/all_to_all | solution.py:431
  55.2 19.5 %all_to_all.40.a_ref = bf16[4,1024,256]{2,1,0:T(8,128)(2,1)S(1)} all-to-all(bf16[4,1024,256]{2,1,0:T(8,128)(2,1)S(1)} %broadcast_in_dim.23), channel_id=1, replica_groups={{0,4,8,12},{1,5,9,13},{2,6,10,14},{3,7,11,15},{16,17,18,19},{20,21,22,2..., dimensions={0} | all-to-all | bytes 4194304 | tf_op jit(solution)/shard_map/all_to_all | solution.py:81
  74.6 2.5 %pre.1 = bf16[4,192,1024]{2,1,0:T(8,128)(2,1)S(1)} custom-call(s32[64]{0:T(128)S(1)} %dynamic-slice_bitcast_fusion.at_ref, bf16[4,1024,256]{2,1,0:T(8,128)(2,1)S(1)} %all_to_all.40.a_ref, bf16[320,512]{1,0:T(8,128)(2,1)S(1)} %get-tuple-element.77.r0.w0, bf16[320,512]{1,0:T(8,128)(2,1)S(1)} %collective-permute-done.r1.w1, ...), custom_call_target="tpu_custom_call" | custom-call | flops 800000000 | bytes 4400000 | tf_op jit(solution)/shard_map/pre/pallas_call | solution.py:438
  77.1 16.4 %all_to_all.41.p_ref = bf16[4,192,1024]{2,1,0:T(8,128)(2,1)S(1)} all-to-all(bf16[4,192,1024]{2,1,0:T(8,128)(2,1)S(1)} %pre.1), channel_id=1, replica_groups={{0,1,2,3},{4,5,6,7},{8,9,10,11},{12,13,14,15},{16,20,24,28},{17,21,25,2..., dimensions={0} | all-to-all | bytes 3145728 | tf_op jit(solution)/shard_map/all_to_all | solution.py:81
  94.4 15.3 %all_to_all.42.h_ref = bf16[4,192,1024]{2,1,0:T(8,128)(2,1)S(1)} all-to-all(bf16[4,192,1024]{2,1,0:T(8,128)(2,1)S(1)} %gates.1), channel_id=1, replica_groups={{0,1,2,3},{4,5,6,7},{8,9,10,11},{12,13,14,15},{16,20,24,28},{17,21,25,2..., dimensions={0} | all-to-all | bytes 3145728 | tf_op jit(solution)/shard_map/all_to_all | solution.py:81
  111.9 12.5 %all_to_all.43.p_ref = bf16[4,1024,128]{2,1,0:T(8,128)(2,1)S(1)} all-to-all(bf16[4,1024,128]{2,1,0:T(8,128)(2,1)S(1)} %partial.1), channel_id=1, replica_groups={{0,4,8,12},{1,5,9,13},{2,6,10,14},{3,7,11,15},{16,17,18,19},{20,21,22,2..., dimensions={0} | all-to-all | bytes 2097152 | tf_op jit(solution)/shard_map/all_to_all | solution.py:81
  125.2 13.6 %all-to-all-start.5 = ((bf16[32,32,128]{2,1,0:T(8,128)(2,1)}), bf16[32,32,128]{2,1,0:T(8,128)(2,1)S(1)}, u32[]{:S(2)}, u32[]{:S(2)}) async-start(bf16[32,32,128]{2,1,0:T(8,128)(2,1)} %bitcast.12), calls=%async_computation.5 | async-start | bytes 524288 | tf_op jit(solution)/shard_map/all_to_all | solution.py:484
  141.2 4.0 %collective-permute-start.6 = (bf16[256,512]{1,0:T(8,128)(2,1)}, bf16[256,512]{1,0:T(8,128)(2,1)S(1)}, u32[]{:S(2)}, u32[]{:S(2)}) collective-permute-start(bf16[256,512]{1,0:T(8,128)(2,1)} %copy-done.17), channel_id=1, source_target_pairs={{0,12},{4,0},{8,4},{12,8},{1,13},{5,1},{9,5},{13,9},{2,14},{6,2},{... | collective-permute-start | bytes 786440 | tf_op jit(solution)/shard_map/ppermute | solution.py:69
  151.0 5.5 %collective-permute-done.4.s1 = bf16[192,512]{1,0:T(8,128)(2,1)S(1)} collective-permute-done((bf16[192,512]{1,0:T(8,128)(2,1)S(1)}, bf16[192,512]{1,0:T(8,128)(2,1)S(1)}, u32[]{:S(2)}, u32[]{:S(2)}) %collective-permute-start.4) | collective-permute-done | bytes 196640 | tf_op jit(solution)/shard_map/ppermute | solution.py:69
  156.4 4.6 %all-to-all-done.5 = bf16[32,32,128]{2,1,0:T(8,128)(2,1)S(1)} async-done(((bf16[32,32,128]{2,1,0:T(8,128)(2,1)}), bf16[32,32,128]{2,1,0:T(8,128)(2,1)S(1)}, u32[]{:S(2)}, u32[]{:S(2)}) %all-to-all-start.5) | async-done | bytes 262176 | tf_op jit(solution)/shard_map/all_to_all | solution.py:484
  163.0 2.6 %collective-permute-start.7 = (bf16[16,64,128]{2,1,0:T(8,128)(2,1)S(1)}, bf16[16,64,128]{2,1,0:T(8,128)(2,1)S(1)}, u32[]{:S(2)}, u32[]{:S(2)}) collective-permute-start(bf16[16,64,128]{2,1,0:T(8,128)(2,1)S(1)} %get-tuple-element.97), channel_id=1, source_target_pairs={{0,16},{16,0},{1,17},{17,1},{2,18},{18,2},{3,19},{19,3},{4,20},{20... | collective-permute-start | bytes 786440 | tf_op jit(solution)/shard_map/ppermute | solution.py:518
  167.3 17.7 %all_to_all.44.r_ref = bf16[16,72,384]{2,1,0:T(8,128)(2,1)S(1)} all-to-all(bf16[16,72,384]{2,1,0:T(8,128)(2,1)S(1)} %join_cores.1), channel_id=1, replica_groups=mesh['z'=16,'c'=2,'y'=4,'x'=4] {'y','x'}, dimensions={0} | all-to-all | bytes 1769472 | tf_op jit(solution)/shard_map/all_to_all | solution.py:543
  185.7 8.3 %all-to-all-start.7 = ((bf16[16,32,128]{2,1,0:T(8,128)(2,1)}), bf16[16,32,128]{2,1,0:T(8,128)(2,1)S(1)}, u32[]{:S(2)}, u32[]{:S(2)}) async-start(bf16[16,32,128]{2,1,0:T(8,128)(2,1)} %proj_part.1), calls=%async_computation.7 | async-start | bytes 262144 | tf_op jit(solution)/shard_map/all_to_all | solution.py:555
  196.5 2.8 %collective-permute-start.9 = (bf16[192,512]{1,0:T(8,128)(2,1)S(1)}, bf16[192,512]{1,0:T(8,128)(2,1)S(1)}, u32[]{:S(2)}, u32[]{:S(2)}) collective-permute-start(bf16[192,512]{1,0:T(8,128)(2,1)S(1)} %copy-done.19), channel_id=1, source_target_pairs={{0,3},{1,0},{2,1},{3,2},{4,7},{5,4},{6,5},{7,6},{8,11},{9,8},{10,9... | collective-permute-start | bytes 589832 | tf_op jit(solution)/shard_map/ppermute | solution.py:69
  199.6 5.2 %collective-permute-start.10 = (f32[64,128]{1,0:T(8,128)S(1)}, f32[64,128]{1,0:T(8,128)S(1)}, u32[]{:S(2)}, u32[]{:S(2)}) collective-permute-start(f32[64,128]{1,0:T(8,128)S(1)} %get-tuple-element.111), channel_id=1, source_target_pairs={{16,0},{32,16},{48,32},{64,48},{80,64},{96,80},{112,96},{128,112},... | collective-permute-start | bytes 98312 | tf_op jit(solution)/shard_map/ppermute | solution.py:576
  204.9 3.3 %collective-permute-done.10.next_ref = f32[64,128]{1,0:T(8,128)S(1)} collective-permute-done((f32[64,128]{1,0:T(8,128)S(1)}, f32[64,128]{1,0:T(8,128)S(1)}, u32[]{:S(2)}, u32[]{:S(2)}) %collective-permute-start.10) | collective-permute-done | bytes 32800 | tf_op jit(solution)/shard_map/ppermute | solution.py:576
  (85 shorter events, 32.2 us)
Async XLA Ops:
  0.6 21.0 %copy-start.6 = (bf16[1,64,2048]{2,1,0:T(8,128)(2,1)S(1)}, bf16[1,64,2048]{2,1,0:T(8,128)(2,1)}, u32[]{:S(2)}) copy-start(bf16[1,64,2048]{2,1,0:T(8,128)(2,1)} %param.18) | copy-start | bytes 786436
  0.7 21.0 %copy-start.7 = (bf16[1,64,2048]{2,1,0:T(8,128)(2,1)S(1)}, bf16[1,64,2048]{2,1,0:T(8,128)(2,1)}, u32[]{:S(2)}) copy-start(bf16[1,64,2048]{2,1,0:T(8,128)(2,1)} %param.19) | copy-start | bytes 786436
  0.7 21.0 %copy-start.8 = (bf16[1,64,2048]{2,1,0:T(8,128)(2,1)S(1)}, bf16[1,64,2048]{2,1,0:T(8,128)(2,1)}, u32[]{:S(2)}) copy-start(bf16[1,64,2048]{2,1,0:T(8,128)(2,1)} %param.20) | copy-start | bytes 786436
  3.6 50.4 %all-to-all-start = ((bf16[32,32,256]{2,1,0:T(8,128)(2,1)}), bf16[32,32,256]{2,1,0:T(8,128)(2,1)}, u32[]{:S(2)}, u32[]{:S(2)}) async-start(bf16[32,32,256]{2,1,0:T(8,128)(2,1)} %bitcast.36), calls=%async_computation | async-start | bytes 1048576 | tf_op jit(solution)/shard_map/all_to_all | solution.py:431
  22.5 10.7 %collective-permute-start = (bf16[320,512]{1,0:T(8,128)(2,1)S(1)}, bf16[320,512]{1,0:T(8,128)(2,1)S(1)}, u32[]{:S(2)}, u32[]{:S(2)}) collective-permute-start(bf16[320,512]{1,0:T(8,128)(2,1)S(1)} %get-tuple-element.69), channel_id=1, source_target_pairs={{0,1},{1,2},{2,3},{3,0},{4,5},{5,6},{6,7},{7,4},{8,9},{9,10},{10,1... | collective-permute-start | bytes 983048 | tf_op jit(solution)/shard_map/ppermute | solution.py:69
  25.7 10.9 %collective-permute-start.1 = (bf16[320,512]{1,0:T(8,128)(2,1)S(1)}, bf16[320,512]{1,0:T(8,128)(2,1)S(1)}, u32[]{:S(2)}, u32[]{:S(2)}) collective-permute-start(bf16[320,512]{1,0:T(8,128)(2,1)S(1)} %get-tuple-element.70), channel_id=1, source_target_pairs={{0,2},{1,3},{2,0},{3,1},{4,6},{5,7},{6,4},{7,5},{8,10},{9,11},{10,... | collective-permute-start | bytes 983048 | tf_op jit(solution)/shard_map/ppermute | solution.py:69
  30.2 8.2 %collective-permute-start.2 = (bf16[320,512]{1,0:T(8,128)(2,1)S(1)}, bf16[320,512]{1,0:T(8,128)(2,1)S(1)}, u32[]{:S(2)}, u32[]{:S(2)}) collective-permute-start(bf16[320,512]{1,0:T(8,128)(2,1)S(1)} %get-tuple-element.71), channel_id=1, source_target_pairs={{0,3},{1,0},{2,1},{3,2},{4,7},{5,4},{6,5},{7,6},{8,11},{9,8},{10,9... | collective-permute-start | bytes 983048 | tf_op jit(solution)/shard_map/ppermute | solution.py:69
  41.2 8.6 %collective-permute-start.3 = (bf16[256,512]{1,0:T(8,128)(2,1)S(1)}, bf16[256,512]{1,0:T(8,128)(2,1)S(1)}, u32[]{:S(2)}, u32[]{:S(2)}) collective-permute-start(bf16[256,512]{1,0:T(8,128)(2,1)S(1)} %get-tuple-element.73), channel_id=1, source_target_pairs={{0,4},{4,8},{8,12},{12,0},{1,5},{5,9},{9,13},{13,1},{2,6},{6,10},{... | collective-permute-start | bytes 786440 | tf_op jit(solution)/shard_map/ppermute | solution.py:69
  125.2 35.9 %copy-start.3 = (bf16[256,512]{1,0:T(8,128)(2,1)S(1)}, bf16[256,512]{1,0:T(8,128)(2,1)}, u32[]{:S(2)}) copy-start(bf16[256,512]{1,0:T(8,128)(2,1)} %copy-done.2) | copy-start | bytes 786436
  125.2 35.9 %copy-start.5 = (bf16[256,512]{1,0:T(8,128)(2,1)S(1)}, bf16[256,512]{1,0:T(8,128)(2,1)}, u32[]{:S(2)}) copy-start(bf16[256,512]{1,0:T(8,128)(2,1)} %copy-done.4) | copy-start | bytes 786436
  125.2 35.9 %all-to-all-start.5 = ((bf16[32,32,128]{2,1,0:T(8,128)(2,1)}), bf16[32,32,128]{2,1,0:T(8,128)(2,1)S(1)}, u32[]{:S(2)}, u32[]{:S(2)}) async-start(bf16[32,32,128]{2,1,0:T(8,128)(2,1)} %bitcast.12), calls=%async_computation.5 | async-start | bytes 524288 | tf_op jit(solution)/shard_map/all_to_all | solution.py:484
  138.8 22.3 %collective-permute-start.5 = (bf16[256,512]{1,0:T(8,128)(2,1)}, bf16[256,512]{1,0:T(8,128)(2,1)S(1)}, u32[]{:S(2)}, u32[]{:S(2)}) collective-permute-start(bf16[256,512]{1,0:T(8,128)(2,1)} %get-tuple-element.92), channel_id=1, source_target_pairs={{0,8},{4,12},{8,0},{12,4},{1,9},{5,13},{9,1},{13,5},{2,10},{6,14},... | collective-permute-start | bytes 786440 | tf_op jit(solution)/shard_map/ppermute | solution.py:69
  141.2 19.8 %collective-permute-start.6 = (bf16[256,512]{1,0:T(8,128)(2,1)}, bf16[256,512]{1,0:T(8,128)(2,1)S(1)}, u32[]{:S(2)}, u32[]{:S(2)}) collective-permute-start(bf16[256,512]{1,0:T(8,128)(2,1)} %copy-done.17), channel_id=1, source_target_pairs={{0,12},{4,0},{8,4},{12,8},{1,13},{5,1},{9,5},{13,9},{2,14},{6,2},{... | collective-permute-start | bytes 786440 | tf_op jit(solution)/shard_map/ppermute | solution.py:69
  148.5 7.9 %collective-permute-start.4 = (bf16[192,512]{1,0:T(8,128)(2,1)S(1)}, bf16[192,512]{1,0:T(8,128)(2,1)S(1)}, u32[]{:S(2)}, u32[]{:S(2)}) collective-permute-start(bf16[192,512]{1,0:T(8,128)(2,1)S(1)} %get-tuple-element.86), channel_id=1, source_target_pairs={{0,1},{1,2},{2,3},{3,0},{4,5},{5,6},{6,7},{7,4},{8,9},{9,10},{10,1... | collective-permute-start | bytes 589832 | tf_op jit(solution)/shard_map/ppermute | solution.py:69
  163.0 4.1 %collective-permute-start.7 = (bf16[16,64,128]{2,1,0:T(8,128)(2,1)S(1)}, bf16[16,64,128]{2,1,0:T(8,128)(2,1)S(1)}, u32[]{:S(2)}, u32[]{:S(2)}) collective-permute-start(bf16[16,64,128]{2,1,0:T(8,128)(2,1)S(1)} %get-tuple-element.97), channel_id=1, source_target_pairs={{0,16},{16,0},{1,17},{17,1},{2,18},{18,2},{3,19},{19,3},{4,20},{20... | collective-permute-start | bytes 786440 | tf_op jit(solution)/shard_map/ppermute | solution.py:518
  167.2 26.8 %copy-start.21 = (bf16[192,512]{1,0:T(8,128)(2,1)S(1)}, bf16[192,512]{1,0:T(8,128)(2,1)}, u32[]{:S(2)}) copy-start(bf16[192,512]{1,0:T(8,128)(2,1)} %copy-done.20) | copy-start | bytes 589828
  167.3 29.2 %copy-start.19 = (bf16[192,512]{1,0:T(8,128)(2,1)S(1)}, bf16[192,512]{1,0:T(8,128)(2,1)}, u32[]{:S(2)}) copy-start(bf16[192,512]{1,0:T(8,128)(2,1)} %copy-done.18) | copy-start | bytes 589828
  185.0 23.2 %copy-start.14 = (bf16[320,64]{0,1:T(8,128)(2,1)S(1)}, bf16[320,64]{0,1:T(8,128)(2,1)}, u32[]{:S(2)}) copy-start(bf16[320,64]{0,1:T(8,128)(2,1)} %param.22) | copy-start | bytes 122884
  185.0 23.2 %copy-start.15 = (bf16[320,64]{0,1:T(8,128)(2,1)S(1)}, bf16[320,64]{0,1:T(8,128)(2,1)}, u32[]{:S(2)}) copy-start(bf16[320,64]{0,1:T(8,128)(2,1)} %param.21) | copy-start | bytes 122884
  185.0 25.1 %copy-start.12 = (bf16[192,512]{1,0:T(8,128)(2,1)S(1)}, bf16[192,512]{1,0:T(8,128)(2,1)}, u32[]{:S(2)}) copy-start(bf16[192,512]{1,0:T(8,128)(2,1)} %copy-done.11) | copy-start | bytes 589828
  185.7 26.2 %all-to-all-start.7 = ((bf16[16,32,128]{2,1,0:T(8,128)(2,1)}), bf16[16,32,128]{2,1,0:T(8,128)(2,1)S(1)}, u32[]{:S(2)}, u32[]{:S(2)}) async-start(bf16[16,32,128]{2,1,0:T(8,128)(2,1)} %proj_part.1), calls=%async_computation.7 | async-start | bytes 262144 | tf_op jit(solution)/shard_map/all_to_all | solution.py:555
  194.0 16.0 %collective-permute-start.8 = (bf16[192,512]{1,0:T(8,128)(2,1)S(1)}, bf16[192,512]{1,0:T(8,128)(2,1)S(1)}, u32[]{:S(2)}, u32[]{:S(2)}) collective-permute-start(bf16[192,512]{1,0:T(8,128)(2,1)S(1)} %copy-done.21), channel_id=1, source_target_pairs={{0,2},{1,3},{2,0},{3,1},{4,6},{5,7},{6,4},{7,5},{8,10},{9,11},{10,... | collective-permute-start | bytes 589832 | tf_op jit(solution)/shard_map/ppermute | solution.py:69
  196.5 13.6 %collective-permute-start.9 = (bf16[192,512]{1,0:T(8,128)(2,1)S(1)}, bf16[192,512]{1,0:T(8,128)(2,1)S(1)}, u32[]{:S(2)}, u32[]{:S(2)}) collective-permute-start(bf16[192,512]{1,0:T(8,128)(2,1)S(1)} %copy-done.19), channel_id=1, source_target_pairs={{0,3},{1,0},{2,1},{3,2},{4,7},{5,4},{6,5},{7,6},{8,11},{9,8},{10,9... | collective-permute-start | bytes 589832 | tf_op jit(solution)/shard_map/ppermute | solution.py:69
  199.6 8.6 %collective-permute-start.10 = (f32[64,128]{1,0:T(8,128)S(1)}, f32[64,128]{1,0:T(8,128)S(1)}, u32[]{:S(2)}, u32[]{:S(2)}) collective-permute-start(f32[64,128]{1,0:T(8,128)S(1)} %get-tuple-element.111), channel_id=1, source_target_pairs={{16,0},{32,16},{48,32},{64,48},{80,64},{96,80},{112,96},{128,112},... | collective-permute-start | bytes 98312 | tf_op jit(solution)/shard_map/ppermute | solution.py:576
  (14 other events, 112.1 us)
where the time goes:
time: 214 us; the launch traced here: 213 us
  blocking collectives  81.4 us (38%)
  starting transfers between devices  74.2 us (35%)
  waiting for transfers between devices  27.5 us (13%)
  Pallas kernels  22.5 us (11%)
  local copies, waits for them, and re-layouts  6.11 us (3%)
    all_to_all x4, blocking collectives, exchange(): return lax.all_to_all(v, PLANE, 0, 0, axis_index_groups=groups, tiled=True)  63.6 us
    ppermute x9, starting transfers between devices, shift(): return lax.ppermute(part, PLANE, steps_ahead(groups, k))  27.7 us
    all_to_all x1, blocking collectives, body(): act_part = lax.all_to_all(act_part, TP, 0, 0, tiled=True)  17.7 us
    all_to_all x1, starting transfers between devices, body(): lax.all_to_all(sent.reshape(sp_count, SLOT, 256), SP, 0, 0, tiled=True)  16.8 us
    ppermute x9, waiting for transfers between devices, shift(): return lax.ppermute(part, PLANE, steps_ahead(groups, k))  16.2 us
    all_to_all x1, starting transfers between devices, body(): returned = lax.all_to_all(back, SP, 0, 0, tiled=True).reshape(slots, 128)  13.6 us
    all_to_all x1, starting transfers between devices, body(): proj_part = lax.all_to_all(proj_part, 'z', 0, 0, tiled=True)  8.28 us
    ppermute x1, starting transfers between devices, body(): after = lax.ppermute(head, SP, behind)  5.19 us
  transfers between devices with their start and end apart: 14, of which 7 were waited for; matrix products, arithmetic and copies ran while one was open for 1% of the time, Pallas kernels for 5%

commit v1 on v0

--- a/solution.py
+++ b/solution.py
@@ -427,10 +427,9 @@
         cost_estimate=cost(1000000, 2000000),
         name="relay",
     )(at, *weights)
-    arrived = shift(relay[1], feature_groups, 1)
     got = lax.all_to_all(sent.reshape(sp_count, SLOT, 256), SP, 0, 0, tiled=True)
     got = got.reshape(slots, 256)
-    got, weights, relay, arrived = lax.optimization_barrier((got, weights, relay, arrived))
+    got, weights, relay = lax.optimization_barrier((got, weights, relay))
     taps_t = conv_taps.T
 
     rows = exchange(jnp.broadcast_to(got[None], (SIDE, slots, 256)), feature_groups)
@@ -480,7 +479,7 @@
         name="sum_side",
     )(part).reshape(sp_count, SLOT, 128)
     back, relay = lax.optimization_barrier((back, relay))
-    relay = (relay[0], arrived, shift(relay[2], feature_groups, 2), shift(relay[3], feature_groups, 3))
+    relay = pass_on(relay, feature_groups)
     returned = lax.all_to_all(back, SP, 0, 0, tiled=True).reshape(slots, 128)
 
     grads = pl.pallas_call(
@@ -497,8 +496,7 @@
         cost_estimate=cost(800000000, 4400000),
         name="grads",
     )(at, hidden, rows)
-    first_grad = shift(grads[1], unit_groups, 1)
-    returned, grads, first_grad = lax.optimization_barrier((returned, grads, first_grad))
+    returned, grads = lax.optimization_barrier((returned, grads))
 
     wide = 384
     mine, other, total_cot, stats = pl.pallas_call(
@@ -540,6 +538,7 @@
         cost_estimate=cost(100000, 1200000),
         name="join_cores",
     )(act_part, mine, other)
+    act_part, grads = lax.optimization_barrier((act_part, grads))
     act_part = lax.all_to_all(act_part, TP, 0, 0, tiled=True)
     proj_part = pl.pallas_call(
         part_kernel,
@@ -550,8 +549,9 @@
         cost_estimate=cost(100000, 400000),
         name="proj_part",
     )(act_part)
-    act_part, proj_part, grads = lax.optimization_barrier((act_part, proj_part, grads))
-    grads = (grads[0], first_grad, shift(grads[2], unit_groups, 2), shift(grads[3], unit_groups, 3))
+    near = [shift(grads[k], unit_groups, k) for k in (1, 3)]
+    act_part, proj_part, last = lax.optimization_barrier((act_part, proj_part, grads[2]))
+    grads = (grads[0], near[0], shift(last, unit_groups, 2), near[1])
     proj_part = lax.all_to_all(proj_part, "z", 0, 0, tiled=True)
     grad_proj = pl.pallas_call(
         sum_kernel,

time: 214 us -> 210 us (0.981)
  starting transfers between devices: 74.2 us -> 66.7 us
    ppermute x9, waiting for transfers between devices: 16.2 us -> 5.24 us  [shift(): return lax.ppermute(part, PLANE, steps_ahead(groups, k))]
    all_to_all x1, waiting for transfers between devices: 3.43 us -> 13.3 us  [body(): lax.all_to_all(sent.reshape(sp_count, SLOT, 256), SP, 0, 0, tiled=True)]
    all_to_all x1, starting transfers between devices: 13.6 us -> 9.08 us  [body(): returned = lax.all_to_all(back, SP, 0, 0, tiled=True).reshape(slots, 128)]
    all_to_all x1, starting transfers between devices: 8.28 us -> 5.67 us  [body(): proj_part = lax.all_to_all(proj_part, 'z', 0, 0, tiled=True)]
    all_to_all x1, waiting for transfers between devices: 4.59 us -> 7.09 us  [body(): returned = lax.all_to_all(back, SP, 0, 0, tiled=True).reshape(slots, 128)]
    unnamed x49 -> x47, local copies, waits for them, and re-layouts: 3.69 us -> 4.99 us
  transfers between devices with their start and end apart: 14 -> 14, of which waited for: 7 -> 5; matrix products, arithmetic and copies ran while one was open for 1% -> 1% of each run, Pallas kernels for 5% -> 5%
where the time goes in v1:
time: 210 us; the launch traced here: 209 us
  blocking collectives  81.3 us (39%)
  starting transfers between devices  66.7 us (32%)
  waiting for transfers between devices  28.9 us (14%)
  Pallas kernels  23.7 us (11%)
  local copies, waits for them, and re-layouts  7.41 us (4%)
    all_to_all x4, blocking collectives, exchange(): return lax.all_to_all(v, PLANE, 0, 0, axis_index_groups=groups, tiled=True)  63.6 us
    ppermute x9, starting transfers between devices, shift(): return lax.ppermute(part, PLANE, steps_ahead(groups, k))  27.5 us
    all_to_all x1, blocking collectives, body(): act_part = lax.all_to_all(act_part, TP, 0, 0, tiled=True)  17.7 us
    all_to_all x1, starting transfers between devices, body(): lax.all_to_all(sent.reshape(sp_count, SLOT, 256), SP, 0, 0, tiled=True)  16.8 us
    all_to_all x1, waiting for transfers between devices, body(): lax.all_to_all(sent.reshape(sp_count, SLOT, 256), SP, 0, 0, tiled=True)  13.3 us
    all_to_all x1, starting transfers between devices, body(): returned = lax.all_to_all(back, SP, 0, 0, tiled=True).reshape(slots, 128)  9.08 us
    all_to_all x1, waiting for transfers between devices, body(): returned = lax.all_to_all(back, SP, 0, 0, tiled=True).reshape(slots, 128)  7.09 us
    all_to_all x1, starting transfers between devices, body(): proj_part = lax.all_to_all(proj_part, 'z', 0, 0, tiled=True)  5.67 us
  transfers between devices with their start and end apart: 14, of which 5 were waited for; matrix products, arithmetic and copies ran while one was open for 1% of the time, Pallas kernels for 5%

profile of v1, /device:TPU:1, one launch (start us, length us, event | category | flops | bytes accessed | tf_op | source)
XLA Modules:
  0.0 209.2 jit_solution(12719681191418152908)
XLA Ops:
  0.7 2.9 %route.1 = (bf16[1024,256]{1,0:T(8,128)(2,1)}, s32[2,320]{1,0:T(2,128)}) custom-call(s32[2,320]{1,0:T(2,128)} %bitcast.42, f32[2,320]{1,0:T(2,128)} %bitcast.43, bf16[320,128]{1,0:T(8,128)(2,1)} %x_ref.1, bf16[320,128]{1,0:T(8,128)(2,1)} %c_ref.3), custom_call_target="tpu_custom_call" | custom-call | flops 400000000 | bytes 2000000 | tf_op jit(solution)/shard_map/route/pallas_call | solution.py:382
  3.6 16.8 %all-to-all-start = ((bf16[32,32,256]{2,1,0:T(8,128)(2,1)}), bf16[32,32,256]{2,1,0:T(8,128)(2,1)}, u32[]{:S(2)}, u32[]{:S(2)}) async-start(bf16[32,32,256]{2,1,0:T(8,128)(2,1)} %bitcast.35), calls=%async_computation | async-start | bytes 1048576 | tf_op jit(solution)/shard_map/all_to_all | solution.py:430
  22.5 3.2 %collective-permute-start = (bf16[320,512]{1,0:T(8,128)(2,1)S(1)}, bf16[320,512]{1,0:T(8,128)(2,1)S(1)}, u32[]{:S(2)}, u32[]{:S(2)}) collective-permute-start(bf16[320,512]{1,0:T(8,128)(2,1)S(1)} %get-tuple-element.73), channel_id=1, source_target_pairs={{0,1},{1,2},{2,3},{3,0},{4,5},{5,6},{6,7},{7,4},{8,9},{9,10},{10,1... | collective-permute-start | bytes 983048 | tf_op jit(solution)/shard_map/ppermute | solution.py:69
  25.7 4.5 %collective-permute-start.1 = (bf16[320,512]{1,0:T(8,128)(2,1)S(1)}, bf16[320,512]{1,0:T(8,128)(2,1)S(1)}, u32[]{:S(2)}, u32[]{:S(2)}) collective-permute-start(bf16[320,512]{1,0:T(8,128)(2,1)S(1)} %get-tuple-element.74), channel_id=1, source_target_pairs={{0,2},{1,3},{2,0},{3,1},{4,6},{5,7},{6,4},{7,5},{8,10},{9,11},{10,... | collective-permute-start | bytes 983048 | tf_op jit(solution)/shard_map/ppermute | solution.py:69
  30.2 3.0 %collective-permute-start.2 = (bf16[320,512]{1,0:T(8,128)(2,1)S(1)}, bf16[320,512]{1,0:T(8,128)(2,1)S(1)}, u32[]{:S(2)}, u32[]{:S(2)}) collective-permute-start(bf16[320,512]{1,0:T(8,128)(2,1)S(1)} %get-tuple-element.75), channel_id=1, source_target_pairs={{0,3},{1,0},{2,1},{3,2},{4,7},{5,4},{6,5},{7,6},{8,11},{9,8},{10,9... | collective-permute-start | bytes 983048 | tf_op jit(solution)/shard_map/ppermute | solution.py:69
  33.2 3.3 %collective-permute-done.1.r2.w2 = bf16[320,512]{1,0:T(8,128)(2,1)S(1)} collective-permute-done((bf16[320,512]{1,0:T(8,128)(2,1)S(1)}, bf16[320,512]{1,0:T(8,128)(2,1)S(1)}, u32[]{:S(2)}, u32[]{:S(2)}) %collective-permute-start.1) | collective-permute-done | bytes 327712 | tf_op jit(solution)/shard_map/ppermute | solution.py:69
  40.7 13.3 %all-to-all-done = bf16[32,32,256]{2,1,0:T(8,128)(2,1)} async-done(((bf16[32,32,256]{2,1,0:T(8,128)(2,1)}), bf16[32,32,256]{2,1,0:T(8,128)(2,1)}, u32[]{:S(2)}, u32[]{:S(2)}) %all-to-all-start) | async-done | bytes 524320 | tf_op jit(solution)/shard_map/all_to_all | solution.py:430
  55.2 19.5 %all_to_all.40.a_ref = bf16[4,1024,256]{2,1,0:T(8,128)(2,1)S(1)} all-to-all(bf16[4,1024,256]{2,1,0:T(8,128)(2,1)S(1)} %broadcast_in_dim.23), channel_id=1, replica_groups={{0,4,8,12},{1,5,9,13},{2,6,10,14},{3,7,11,15},{16,17,18,19},{20,21,22,2..., dimensions={0} | all-to-all | bytes 4194304 | tf_op jit(solution)/shard_map/all_to_all | solution.py:81
  74.6 2.5 %pre.1 = bf16[4,192,1024]{2,1,0:T(8,128)(2,1)S(1)} custom-call(s32[64]{0:T(128)S(1)} %dynamic-slice_bitcast_fusion.at_ref, bf16[4,1024,256]{2,1,0:T(8,128)(2,1)S(1)} %all_to_all.40.a_ref, bf16[320,512]{1,0:T(8,128)(2,1)S(1)} %get-tuple-element.81.r0.w0, bf16[320,512]{1,0:T(8,128)(2,1)S(1)} %collective-permute-done.r1.w1, ...), custom_call_target="tpu_custom_call" | custom-call | flops 800000000 | bytes 4400000 | tf_op jit(solution)/shard_map/pre/pallas_call | solution.py:437
  77.2 16.4 %all_to_all.41.p_ref = bf16[4,192,1024]{2,1,0:T(8,128)(2,1)S(1)} all-to-all(bf16[4,192,1024]{2,1,0:T(8,128)(2,1)S(1)} %pre.1), channel_id=1, replica_groups={{0,1,2,3},{4,5,6,7},{8,9,10,11},{12,13,14,15},{16,20,24,28},{17,21,25,2..., dimensions={0} | all-to-all | bytes 3145728 | tf_op jit(solution)/shard_map/all_to_all | solution.py:81
  94.4 15.3 %all_to_all.42.h_ref = bf16[4,192,1024]{2,1,0:T(8,128)(2,1)S(1)} all-to-all(bf16[4,192,1024]{2,1,0:T(8,128)(2,1)S(1)} %gates.1), channel_id=1, replica_groups={{0,1,2,3},{4,5,6,7},{8,9,10,11},{12,13,14,15},{16,20,24,28},{17,21,25,2..., dimensions={0} | all-to-all | bytes 3145728 | tf_op jit(solution)/shard_map/all_to_all | solution.py:81
  111.9 12.5 %all_to_all.43.p_ref = bf16[4,1024,128]{2,1,0:T(8,128)(2,1)S(1)} all-to-all(bf16[4,1024,128]{2,1,0:T(8,128)(2,1)S(1)} %partial.1), channel_id=1, replica_groups={{0,4,8,12},{1,5,9,13},{2,6,10,14},{3,7,11,15},{16,17,18,19},{20,21,22,2..., dimensions={0} | all-to-all | bytes 2097152 | tf_op jit(solution)/shard_map/all_to_all | solution.py:81
  125.2 9.1 %all-to-all-start.5 = ((bf16[32,32,128]{2,1,0:T(8,128)(2,1)}), bf16[32,32,128]{2,1,0:T(8,128)(2,1)}, u32[]{:S(2)}, u32[]{:S(2)}) async-start(bf16[32,32,128]{2,1,0:T(8,128)(2,1)} %bitcast.12), calls=%async_computation.5 | async-start | bytes 524288 | tf_op jit(solution)/shard_map/all_to_all | solution.py:483
  134.3 2.2 %collective-permute-start.3 = (bf16[256,512]{1,0:T(8,128)(2,1)}, bf16[256,512]{1,0:T(8,128)(2,1)S(1)}, u32[]{:S(2)}, u32[]{:S(2)}) collective-permute-start(bf16[256,512]{1,0:T(8,128)(2,1)} %get-tuple-element.96), channel_id=1, source_target_pairs={{0,4},{4,8},{8,12},{12,0},{1,5},{5,9},{9,13},{13,1},{2,6},{6,10},{... | collective-permute-start | bytes 786440 | tf_op jit(solution)/shard_map/ppermute | solution.py:69
  136.5 3.7 %collective-permute-start.4 = (bf16[256,512]{1,0:T(8,128)(2,1)}, bf16[256,512]{1,0:T(8,128)(2,1)}, u32[]{:S(2)}, u32[]{:S(2)}) collective-permute-start(bf16[256,512]{1,0:T(8,128)(2,1)} %get-tuple-element.97), channel_id=1, source_target_pairs={{0,8},{4,12},{8,0},{12,4},{1,9},{5,13},{9,1},{13,5},{2,10},{6,14},... | collective-permute-start | bytes 786440 | tf_op jit(solution)/shard_map/ppermute | solution.py:69
  140.2 2.5 %collective-permute-start.5 = (bf16[256,512]{1,0:T(8,128)(2,1)}, bf16[256,512]{1,0:T(8,128)(2,1)}, u32[]{:S(2)}, u32[]{:S(2)}) collective-permute-start(bf16[256,512]{1,0:T(8,128)(2,1)} %get-tuple-element.98), channel_id=1, source_target_pairs={{0,12},{4,0},{8,4},{12,8},{1,13},{5,1},{9,5},{13,9},{2,14},{6,2},{... | collective-permute-start | bytes 786440 | tf_op jit(solution)/shard_map/ppermute | solution.py:69
  148.9 7.1 %all-to-all-done.5 = bf16[32,32,128]{2,1,0:T(8,128)(2,1)} async-done(((bf16[32,32,128]{2,1,0:T(8,128)(2,1)}), bf16[32,32,128]{2,1,0:T(8,128)(2,1)}, u32[]{:S(2)}, u32[]{:S(2)}) %all-to-all-start.5) | async-done | bytes 262176 | tf_op jit(solution)/shard_map/all_to_all | solution.py:483
  156.0 2.5 %total_cot.1 = (bf16[16,64,128]{2,1,0:T(8,128)(2,1)S(1)}, bf16[16,64,128]{2,1,0:T(8,128)(2,1)S(1)}, bf16[384,128]{1,0:T(8,128)(2,1)S(1)}, f32[2,320]{1,0:T(2,128)S(1)}) custom-call(s32[64]{0:T(128)S(1)} %dynamic-slice_bitcast_fusion.at_ref, bf16[1024,320]{1,0:T(8,128)(2,1)S(1)} %pick.1.p_ref, bf16[1024,128]{1,0:T(8,128)(2,1)} %bitcast.13.r_ref, ...), custom_call_target="tpu_custom_call" | custom-call | flops 170000000 | bytes 2500000 | tf_op jit(solution)/shard_map/total_cot/pallas_call | solution.py:502
  158.5 3.4 %collective-permute-start.6 = (bf16[16,64,128]{2,1,0:T(8,128)(2,1)S(1)}, bf16[16,64,128]{2,1,0:T(8,128)(2,1)S(1)}, u32[]{:S(2)}, u32[]{:S(2)}) collective-permute-start(bf16[16,64,128]{2,1,0:T(8,128)(2,1)S(1)} %get-tuple-element.102), channel_id=1, source_target_pairs={{0,16},{16,0},{1,17},{17,1},{2,18},{18,2},{3,19},{19,3},{4,20},{20... | collective-permute-start | bytes 786440 | tf_op jit(solution)/shard_map/ppermute | solution.py:516
  164.1 17.7 %all_to_all.44.r_ref = bf16[16,72,384]{2,1,0:T(8,128)(2,1)S(1)} all-to-all(bf16[16,72,384]{2,1,0:T(8,128)(2,1)S(1)} %join_cores.1), channel_id=1, replica_groups=mesh['z'=16,'c'=2,'y'=4,'x'=4] {'y','x'}, dimensions={0} | all-to-all | bytes 1769472 | tf_op jit(solution)/shard_map/all_to_all | solution.py:542
  182.6 5.7 %all-to-all-start.7 = ((bf16[16,32,128]{2,1,0:T(8,128)(2,1)}), bf16[16,32,128]{2,1,0:T(8,128)(2,1)S(1)}, u32[]{:S(2)}, u32[]{:S(2)}) async-start(bf16[16,32,128]{2,1,0:T(8,128)(2,1)} %proj_part.1), calls=%async_computation.7 | async-start | bytes 262144 | tf_op jit(solution)/shard_map/all_to_all | solution.py:555
  190.2 4.6 %collective-permute-start.9 = (bf16[192,512]{1,0:T(8,128)(2,1)S(1)}, bf16[192,512]{1,0:T(8,128)(2,1)S(1)}, u32[]{:S(2)}, u32[]{:S(2)}) collective-permute-start(bf16[192,512]{1,0:T(8,128)(2,1)S(1)} %copy-done.18), channel_id=1, source_target_pairs={{0,3},{1,0},{2,1},{3,2},{4,7},{5,4},{6,5},{7,6},{8,11},{9,8},{10,9... | collective-permute-start | bytes 589832 | tf_op jit(solution)/shard_map/ppermute | solution.py:69
  197.0 4.2 %collective-permute-start.10 = (f32[64,128]{1,0:T(8,128)S(1)}, f32[64,128]{1,0:T(8,128)S(1)}, u32[]{:S(2)}, u32[]{:S(2)}) collective-permute-start(f32[64,128]{1,0:T(8,128)S(1)} %get-tuple-element.119), channel_id=1, source_target_pairs={{16,0},{32,16},{48,32},{64,48},{80,64},{96,80},{112,96},{128,112},... | collective-permute-start | bytes 98312 | tf_op jit(solution)/shard_map/ppermute | solution.py:576
  201.3 3.3 %collective-permute-done.10.next_ref = f32[64,128]{1,0:T(8,128)S(1)} collective-permute-done((f32[64,128]{1,0:T(8,128)S(1)}, f32[64,128]{1,0:T(8,128)S(1)}, u32[]{:S(2)}, u32[]{:S(2)}) %collective-permute-start.10) | collective-permute-done | bytes 32800 | tf_op jit(solution)/shard_map/ppermute | solution.py:576
  (83 shorter events, 29.0 us)
Async XLA Ops:
  0.6 21.0 %copy-start.4 = (bf16[1,64,2048]{2,1,0:T(8,128)(2,1)S(1)}, bf16[1,64,2048]{2,1,0:T(8,128)(2,1)}, u32[]{:S(2)}) copy-start(bf16[1,64,2048]{2,1,0:T(8,128)(2,1)} %param.18) | copy-start | bytes 786436
  0.7 21.0 %copy-start.5 = (bf16[1,64,2048]{2,1,0:T(8,128)(2,1)S(1)}, bf16[1,64,2048]{2,1,0:T(8,128)(2,1)}, u32[]{:S(2)}) copy-start(bf16[1,64,2048]{2,1,0:T(8,128)(2,1)} %param.19) | copy-start | bytes 786436
  0.7 21.0 %copy-start.6 = (bf16[1,64,2048]{2,1,0:T(8,128)(2,1)S(1)}, bf16[1,64,2048]{2,1,0:T(8,128)(2,1)}, u32[]{:S(2)}) copy-start(bf16[1,64,2048]{2,1,0:T(8,128)(2,1)} %param.20) | copy-start | bytes 786436
  3.6 50.4 %all-to-all-start = ((bf16[32,32,256]{2,1,0:T(8,128)(2,1)}), bf16[32,32,256]{2,1,0:T(8,128)(2,1)}, u32[]{:S(2)}, u32[]{:S(2)}) async-start(bf16[32,32,256]{2,1,0:T(8,128)(2,1)} %bitcast.35), calls=%async_computation | async-start | bytes 1048576 | tf_op jit(solution)/shard_map/all_to_all | solution.py:430
  22.5 10.7 %collective-permute-start = (bf16[320,512]{1,0:T(8,128)(2,1)S(1)}, bf16[320,512]{1,0:T(8,128)(2,1)S(1)}, u32[]{:S(2)}, u32[]{:S(2)}) collective-permute-start(bf16[320,512]{1,0:T(8,128)(2,1)S(1)} %get-tuple-element.73), channel_id=1, source_target_pairs={{0,1},{1,2},{2,3},{3,0},{4,5},{5,6},{6,7},{7,4},{8,9},{9,10},{10,1... | collective-permute-start | bytes 983048 | tf_op jit(solution)/shard_map/ppermute | solution.py:69
  25.7 10.9 %collective-permute-start.1 = (bf16[320,512]{1,0:T(8,128)(2,1)S(1)}, bf16[320,512]{1,0:T(8,128)(2,1)S(1)}, u32[]{:S(2)}, u32[]{:S(2)}) collective-permute-start(bf16[320,512]{1,0:T(8,128)(2,1)S(1)} %get-tuple-element.74), channel_id=1, source_target_pairs={{0,2},{1,3},{2,0},{3,1},{4,6},{5,7},{6,4},{7,5},{8,10},{9,11},{10,... | collective-permute-start | bytes 983048 | tf_op jit(solution)/shard_map/ppermute | solution.py:69
  30.2 8.2 %collective-permute-start.2 = (bf16[320,512]{1,0:T(8,128)(2,1)S(1)}, bf16[320,512]{1,0:T(8,128)(2,1)S(1)}, u32[]{:S(2)}, u32[]{:S(2)}) collective-permute-start(bf16[320,512]{1,0:T(8,128)(2,1)S(1)} %get-tuple-element.75), channel_id=1, source_target_pairs={{0,3},{1,0},{2,1},{3,2},{4,7},{5,4},{6,5},{7,6},{8,11},{9,8},{10,9... | collective-permute-start | bytes 983048 | tf_op jit(solution)/shard_map/ppermute | solution.py:69
  111.9 30.8 %copy-start.14 = (s32[2,320]{1,0:T(2,128)S(1)}, s32[2,320]{1,0:T(2,128)}, u32[]{:S(2)}) copy-start(s32[2,320]{1,0:T(2,128)} %get-tuple-element.67.t_ref) | copy-start | bytes 7684
  125.2 30.8 %all-to-all-start.5 = ((bf16[32,32,128]{2,1,0:T(8,128)(2,1)}), bf16[32,32,128]{2,1,0:T(8,128)(2,1)}, u32[]{:S(2)}, u32[]{:S(2)}) async-start(bf16[32,32,128]{2,1,0:T(8,128)(2,1)} %bitcast.12), calls=%async_computation.5 | async-start | bytes 524288 | tf_op jit(solution)/shard_map/all_to_all | solution.py:483
  134.3 21.7 %collective-permute-start.3 = (bf16[256,512]{1,0:T(8,128)(2,1)}, bf16[256,512]{1,0:T(8,128)(2,1)S(1)}, u32[]{:S(2)}, u32[]{:S(2)}) collective-permute-start(bf16[256,512]{1,0:T(8,128)(2,1)} %get-tuple-element.96), channel_id=1, source_target_pairs={{0,4},{4,8},{8,12},{12,0},{1,5},{5,9},{9,13},{13,1},{2,6},{6,10},{... | collective-permute-start | bytes 786440 | tf_op jit(solution)/shard_map/ppermute | solution.py:69
  136.5 19.5 %collective-permute-start.4 = (bf16[256,512]{1,0:T(8,128)(2,1)}, bf16[256,512]{1,0:T(8,128)(2,1)}, u32[]{:S(2)}, u32[]{:S(2)}) collective-permute-start(bf16[256,512]{1,0:T(8,128)(2,1)} %get-tuple-element.97), channel_id=1, source_target_pairs={{0,8},{4,12},{8,0},{12,4},{1,9},{5,13},{9,1},{13,5},{2,10},{6,14},... | collective-permute-start | bytes 786440 | tf_op jit(solution)/shard_map/ppermute | solution.py:69
  140.2 15.8 %collective-permute-start.5 = (bf16[256,512]{1,0:T(8,128)(2,1)}, bf16[256,512]{1,0:T(8,128)(2,1)}, u32[]{:S(2)}, u32[]{:S(2)}) collective-permute-start(bf16[256,512]{1,0:T(8,128)(2,1)} %get-tuple-element.98), channel_id=1, source_target_pairs={{0,12},{4,0},{8,4},{12,8},{1,13},{5,1},{9,5},{13,9},{2,14},{6,2},{... | collective-permute-start | bytes 786440 | tf_op jit(solution)/shard_map/ppermute | solution.py:69
  158.5 5.4 %collective-permute-start.6 = (bf16[16,64,128]{2,1,0:T(8,128)(2,1)S(1)}, bf16[16,64,128]{2,1,0:T(8,128)(2,1)S(1)}, u32[]{:S(2)}, u32[]{:S(2)}) collective-permute-start(bf16[16,64,128]{2,1,0:T(8,128)(2,1)S(1)} %get-tuple-element.102), channel_id=1, source_target_pairs={{0,16},{16,0},{1,17},{17,1},{2,18},{18,2},{3,19},{19,3},{4,20},{20... | collective-permute-start | bytes 786440 | tf_op jit(solution)/shard_map/ppermute | solution.py:516
  164.1 24.2 %copy-start.20 = (bf16[192,512]{1,0:T(8,128)(2,1)S(1)}, bf16[192,512]{1,0:T(8,128)(2,1)}, u32[]{:S(2)}) copy-start(bf16[192,512]{1,0:T(8,128)(2,1)} %copy-done.19) | copy-start | bytes 589828
  164.1 26.1 %copy-start.18 = (bf16[192,512]{1,0:T(8,128)(2,1)S(1)}, bf16[192,512]{1,0:T(8,128)(2,1)}, u32[]{:S(2)}) copy-start(bf16[192,512]{1,0:T(8,128)(2,1)} %copy-done.17) | copy-start | bytes 589828
  164.1 30.7 %copy-start.16 = (bf16[192,512]{1,0:T(8,128)(2,1)S(1)}, bf16[192,512]{1,0:T(8,128)(2,1)}, u32[]{:S(2)}) copy-start(bf16[192,512]{1,0:T(8,128)(2,1)} %copy-done.15) | copy-start | bytes 589828
  181.8 22.8 %copy-start.12 = (bf16[320,64]{0,1:T(8,128)(2,1)S(1)}, bf16[320,64]{0,1:T(8,128)(2,1)}, u32[]{:S(2)}) copy-start(bf16[320,64]{0,1:T(8,128)(2,1)} %param.22) | copy-start | bytes 122884
  181.8 22.8 %copy-start.13 = (bf16[320,64]{0,1:T(8,128)(2,1)S(1)}, bf16[320,64]{0,1:T(8,128)(2,1)}, u32[]{:S(2)}) copy-start(bf16[320,64]{0,1:T(8,128)(2,1)} %param.21) | copy-start | bytes 122884
  181.8 24.7 %copy-start.10 = (bf16[192,512]{1,0:T(8,128)(2,1)S(1)}, bf16[192,512]{1,0:T(8,128)(2,1)}, u32[]{:S(2)}) copy-start(bf16[192,512]{1,0:T(8,128)(2,1)} %copy-done.9) | copy-start | bytes 589828
  182.6 25.8 %all-to-all-start.7 = ((bf16[16,32,128]{2,1,0:T(8,128)(2,1)}), bf16[16,32,128]{2,1,0:T(8,128)(2,1)S(1)}, u32[]{:S(2)}, u32[]{:S(2)}) async-start(bf16[16,32,128]{2,1,0:T(8,128)(2,1)} %proj_part.1), calls=%async_computation.7 | async-start | bytes 262144 | tf_op jit(solution)/shard_map/all_to_all | solution.py:555
  188.3 18.2 %collective-permute-start.7 = (bf16[192,512]{1,0:T(8,128)(2,1)S(1)}, bf16[192,512]{1,0:T(8,128)(2,1)S(1)}, u32[]{:S(2)}, u32[]{:S(2)}) collective-permute-start(bf16[192,512]{1,0:T(8,128)(2,1)S(1)} %copy-done.20), channel_id=1, source_target_pairs={{0,1},{1,2},{2,3},{3,0},{4,5},{5,6},{6,7},{7,4},{8,9},{9,10},{10,1... | collective-permute-start | bytes 589832 | tf_op jit(solution)/shard_map/ppermute | solution.py:69
  190.2 16.3 %collective-permute-start.9 = (bf16[192,512]{1,0:T(8,128)(2,1)S(1)}, bf16[192,512]{1,0:T(8,128)(2,1)S(1)}, u32[]{:S(2)}, u32[]{:S(2)}) collective-permute-start(bf16[192,512]{1,0:T(8,128)(2,1)S(1)} %copy-done.18), channel_id=1, source_target_pairs={{0,3},{1,0},{2,1},{3,2},{4,7},{5,4},{6,5},{7,6},{8,11},{9,8},{10,9... | collective-permute-start | bytes 589832 | tf_op jit(solution)/shard_map/ppermute | solution.py:69
  194.8 11.7 %collective-permute-start.8 = (bf16[192,512]{1,0:T(8,128)(2,1)S(1)}, bf16[192,512]{1,0:T(8,128)(2,1)S(1)}, u32[]{:S(2)}, u32[]{:S(2)}) collective-permute-start(bf16[192,512]{1,0:T(8,128)(2,1)S(1)} %copy-done.16), channel_id=1, source_target_pairs={{0,2},{1,3},{2,0},{3,1},{4,6},{5,7},{6,4},{7,5},{8,10},{9,11},{10,... | collective-permute-start | bytes 589832 | tf_op jit(solution)/shard_map/ppermute | solution.py:69
  197.0 7.6 %collective-permute-start.10 = (f32[64,128]{1,0:T(8,128)S(1)}, f32[64,128]{1,0:T(8,128)S(1)}, u32[]{:S(2)}, u32[]{:S(2)}) collective-permute-start(f32[64,128]{1,0:T(8,128)S(1)} %get-tuple-element.119), channel_id=1, source_target_pairs={{16,0},{32,16},{48,32},{64,48},{80,64},{96,80},{112,96},{128,112},... | collective-permute-start | bytes 98312 | tf_op jit(solution)/shard_map/ppermute | solution.py:576
  (13 other events, 110.5 us)

commit v2 on v1

--- a/solution.py
+++ b/solution.py
@@ -284,8 +284,11 @@
     low = lax.broadcasted_iota(jnp.int32, (64, 128), 1) < 64
     for b in range(o_ref.shape[0]):
         piece = mine_ref[b].astype(F32) + other_ref[b].astype(F32)
-        o_ref[b, 0:64, :] = jnp.where(low, a_ref[b, 0:64, :].astype(F32), piece).astype(BF)
-        o_ref[b, 64:72, :] = a_ref[b, 64:72, :]
+        o_ref[b, :, 0:256] = a_ref[b, :, 0:256]
+        o_ref[b, 0:64, 256:384] = jnp.where(
+            low, a_ref[b, 0:64, 256:384].astype(F32), piece
+        ).astype(BF)
+        o_ref[b, 64:72, 256:384] = a_ref[b, 64:72, 256:384]
 
 
 def part_kernel(r_ref, o_ref):
@@ -525,17 +528,16 @@
     )(at, total_cot, stats, *relay)
     act_part = pl.pallas_call(
         join_kernel,
-        grid=(1,),
+        grid=(2,),
         out_shape=whole((tp_count, 72, wide), BF),
         in_specs=[
-            pl.BlockSpec((tp_count, 72, 128), lambda i: (0, 0, 2)),
-            pl.BlockSpec((tp_count, 64, 128), lambda i: (0, 0, 0)),
-            pl.BlockSpec((tp_count, 64, 128), lambda i: (0, 0, 0)),
+            pl.BlockSpec((8, 72, wide), lambda i: (i, 0, 0)),
+            pl.BlockSpec((8, 64, 128), lambda i: (i, 0, 0)),
+            pl.BlockSpec((8, 64, 128), lambda i: (i, 0, 0)),
         ],
-        out_specs=pl.BlockSpec((tp_count, 72, 128), lambda i: (0, 0, 2)),
-        input_output_aliases={0: 0},
-        compiler_params=room,
-        cost_estimate=cost(100000, 1200000),
+        out_specs=pl.BlockSpec((8, 72, wide), lambda i: (i, 0, 0)),
+        compiler_params=room,
+        cost_estimate=cost(100000, 2200000),
         name="join_cores",
     )(act_part, mine, other)
     act_part, grads = lax.optimization_barrier((act_part, grads))

time: 210 us -> 210 us (level)
  no operation moved by 1% of the time
where the time goes in v2:
time: 210 us; the launch traced here: 209 us
  blocking collectives  81.3 us (39%)
  starting transfers between devices  66.7 us (32%)
  waiting for transfers between devices  28.9 us (14%)
  Pallas kernels  23.7 us (11%)
  local copies, waits for them, and re-layouts  7.41 us (4%)
    all_to_all x4, blocking collectives, exchange(): return lax.all_to_all(v, PLANE, 0, 0, axis_index_groups=groups, tiled=True)  63.6 us
    ppermute x9, starting transfers between devices, shift(): return lax.ppermute(part, PLANE, steps_ahead(groups, k))  27.5 us
    all_to_all x1, blocking collectives, body(): act_part = lax.all_to_all(act_part, TP, 0, 0, tiled=True)  17.7 us
    all_to_all x1, starting transfers between devices, body(): lax.all_to_all(sent.reshape(sp_count, SLOT, 256), SP, 0, 0, tiled=True)  16.8 us
    all_to_all x1, waiting for transfers between devices, body(): lax.all_to_all(sent.reshape(sp_count, SLOT, 256), SP, 0, 0, tiled=True)  13.3 us
    all_to_all x1, starting transfers between devices, body(): returned = lax.all_to_all(back, SP, 0, 0, tiled=True).reshape(slots, 128)  9.08 us
    all_to_all x1, waiting for transfers between devices, body(): returned = lax.all_to_all(back, SP, 0, 0, tiled=True).reshape(slots, 128)  7.09 us
    all_to_all x1, starting transfers between devices, body(): proj_part = lax.all_to_all(proj_part, 'z', 0, 0, tiled=True)  5.67 us
  transfers between devices with their start and end apart: 14, of which 5 were waited for; matrix products, arithmetic and copies ran while one was open for 1% of the time, Pallas kernels for 5%

profile of v2, /device:TPU:1, one launch (start us, length us, event | category | flops | bytes accessed | tf_op | source)
XLA Modules:
  0.0 209.2 jit_solution(12584727460232823536)
XLA Ops:
  0.7 2.9 %route.1 = (bf16[1024,256]{1,0:T(8,128)(2,1)}, s32[2,320]{1,0:T(2,128)}) custom-call(s32[2,320]{1,0:T(2,128)} %bitcast.42, f32[2,320]{1,0:T(2,128)} %bitcast.43, bf16[320,128]{1,0:T(8,128)(2,1)} %x_ref.1, bf16[320,128]{1,0:T(8,128)(2,1)} %c_ref.3), custom_call_target="tpu_custom_call" | custom-call | flops 400000000 | bytes 2000000 | tf_op jit(solution)/shard_map/route/pallas_call | solution.py:385
  3.6 16.8 %all-to-all-start = ((bf16[32,32,256]{2,1,0:T(8,128)(2,1)}), bf16[32,32,256]{2,1,0:T(8,128)(2,1)}, u32[]{:S(2)}, u32[]{:S(2)}) async-start(bf16[32,32,256]{2,1,0:T(8,128)(2,1)} %bitcast.35), calls=%async_computation | async-start | bytes 1048576 | tf_op jit(solution)/shard_map/all_to_all | solution.py:433
  22.5 3.2 %collective-permute-start = (bf16[320,512]{1,0:T(8,128)(2,1)S(1)}, bf16[320,512]{1,0:T(8,128)(2,1)S(1)}, u32[]{:S(2)}, u32[]{:S(2)}) collective-permute-start(bf16[320,512]{1,0:T(8,128)(2,1)S(1)} %get-tuple-element.73), channel_id=1, source_target_pairs={{0,1},{1,2},{2,3},{3,0},{4,5},{5,6},{6,7},{7,4},{8,9},{9,10},{10,1... | collective-permute-start | bytes 983048 | tf_op jit(solution)/shard_map/ppermute | solution.py:69
  25.7 4.5 %collective-permute-start.1 = (bf16[320,512]{1,0:T(8,128)(2,1)S(1)}, bf16[320,512]{1,0:T(8,128)(2,1)S(1)}, u32[]{:S(2)}, u32[]{:S(2)}) collective-permute-start(bf16[320,512]{1,0:T(8,128)(2,1)S(1)} %get-tuple-element.74), channel_id=1, source_target_pairs={{0,2},{1,3},{2,0},{3,1},{4,6},{5,7},{6,4},{7,5},{8,10},{9,11},{10,... | collective-permute-start | bytes 983048 | tf_op jit(solution)/shard_map/ppermute | solution.py:69
  30.2 3.0 %collective-permute-start.2 = (bf16[320,512]{1,0:T(8,128)(2,1)S(1)}, bf16[320,512]{1,0:T(8,128)(2,1)S(1)}, u32[]{:S(2)}, u32[]{:S(2)}) collective-permute-start(bf16[320,512]{1,0:T(8,128)(2,1)S(1)} %get-tuple-element.75), channel_id=1, source_target_pairs={{0,3},{1,0},{2,1},{3,2},{4,7},{5,4},{6,5},{7,6},{8,11},{9,8},{10,9... | collective-permute-start | bytes 983048 | tf_op jit(solution)/shard_map/ppermute | solution.py:69
  33.2 3.3 %collective-permute-done.1.r2.w2 = bf16[320,512]{1,0:T(8,128)(2,1)S(1)} collective-permute-done((bf16[320,512]{1,0:T(8,128)(2,1)S(1)}, bf16[320,512]{1,0:T(8,128)(2,1)S(1)}, u32[]{:S(2)}, u32[]{:S(2)}) %collective-permute-start.1) | collective-permute-done | bytes 327712 | tf_op jit(solution)/shard_map/ppermute | solution.py:69
  40.7 13.3 %all-to-all-done = bf16[32,32,256]{2,1,0:T(8,128)(2,1)} async-done(((bf16[32,32,256]{2,1,0:T(8,128)(2,1)}), bf16[32,32,256]{2,1,0:T(8,128)(2,1)}, u32[]{:S(2)}, u32[]{:S(2)}) %all-to-all-start) | async-done | bytes 524320 | tf_op jit(solution)/shard_map/all_to_all | solution.py:433
  55.2 19.5 %all_to_all.40.a_ref = bf16[4,1024,256]{2,1,0:T(8,128)(2,1)S(1)} all-to-all(bf16[4,1024,256]{2,1,0:T(8,128)(2,1)S(1)} %broadcast_in_dim.23), channel_id=1, replica_groups={{0,4,8,12},{1,5,9,13},{2,6,10,14},{3,7,11,15},{16,17,18,19},{20,21,22,2..., dimensions={0} | all-to-all | bytes 4194304 | tf_op jit(solution)/shard_map/all_to_all | solution.py:81
  74.6 2.5 %pre.1 = bf16[4,192,1024]{2,1,0:T(8,128)(2,1)S(1)} custom-call(s32[64]{0:T(128)S(1)} %dynamic-slice_bitcast_fusion.at_ref, bf16[4,1024,256]{2,1,0:T(8,128)(2,1)S(1)} %all_to_all.40.a_ref, bf16[320,512]{1,0:T(8,128)(2,1)S(1)} %get-tuple-element.81.r0.w0, bf16[320,512]{1,0:T(8,128)(2,1)S(1)} %collective-permute-done.r1.w1, ...), custom_call_target="tpu_custom_call" | custom-call | flops 800000000 | bytes 4400000 | tf_op jit(solution)/shard_map/pre/pallas_call | solution.py:440
  77.2 16.4 %all_to_all.41.p_ref = bf16[4,192,1024]{2,1,0:T(8,128)(2,1)S(1)} all-to-all(bf16[4,192,1024]{2,1,0:T(8,128)(2,1)S(1)} %pre.1), channel_id=1, replica_groups={{0,1,2,3},{4,5,6,7},{8,9,10,11},{12,13,14,15},{16,20,24,28},{17,21,25,2..., dimensions={0} | all-to-all | bytes 3145728 | tf_op jit(solution)/shard_map/all_to_all | solution.py:81
  94.4 15.3 %all_to_all.42.h_ref = bf16[4,192,1024]{2,1,0:T(8,128)(2,1)S(1)} all-to-all(bf16[4,192,1024]{2,1,0:T(8,128)(2,1)S(1)} %gates.1), channel_id=1, replica_groups={{0,1,2,3},{4,5,6,7},{8,9,10,11},{12,13,14,15},{16,20,24,28},{17,21,25,2..., dimensions={0} | all-to-all | bytes 3145728 | tf_op jit(solution)/shard_map/all_to_all | solution.py:81
  111.9 12.5 %all_to_all.43.p_ref = bf16[4,1024,128]{2,1,0:T(8,128)(2,1)S(1)} all-to-all(bf16[4,1024,128]{2,1,0:T(8,128)(2,1)S(1)} %partial.1), channel_id=1, replica_groups={{0,4,8,12},{1,5,9,13},{2,6,10,14},{3,7,11,15},{16,17,18,19},{20,21,22,2..., dimensions={0} | all-to-all | bytes 2097152 | tf_op jit(solution)/shard_map/all_to_all | solution.py:81
  125.2 9.1 %all-to-all-start.5 = ((bf16[32,32,128]{2,1,0:T(8,128)(2,1)}), bf16[32,32,128]{2,1,0:T(8,128)(2,1)}, u32[]{:S(2)}, u32[]{:S(2)}) async-start(bf16[32,32,128]{2,1,0:T(8,128)(2,1)} %bitcast.12), calls=%async_computation.5 | async-start | bytes 524288 | tf_op jit(solution)/shard_map/all_to_all | solution.py:486
  134.3 2.2 %collective-permute-start.3 = (bf16[256,512]{1,0:T(8,128)(2,1)}, bf16[256,512]{1,0:T(8,128)(2,1)S(1)}, u32[]{:S(2)}, u32[]{:S(2)}) collective-permute-start(bf16[256,512]{1,0:T(8,128)(2,1)} %get-tuple-element.96), channel_id=1, source_target_pairs={{0,4},{4,8},{8,12},{12,0},{1,5},{5,9},{9,13},{13,1},{2,6},{6,10},{... | collective-permute-start | bytes 786440 | tf_op jit(solution)/shard_map/ppermute | solution.py:69
  136.5 3.7 %collective-permute-start.4 = (bf16[256,512]{1,0:T(8,128)(2,1)}, bf16[256,512]{1,0:T(8,128)(2,1)}, u32[]{:S(2)}, u32[]{:S(2)}) collective-permute-start(bf16[256,512]{1,0:T(8,128)(2,1)} %get-tuple-element.97), channel_id=1, source_target_pairs={{0,8},{4,12},{8,0},{12,4},{1,9},{5,13},{9,1},{13,5},{2,10},{6,14},... | collective-permute-start | bytes 786440 | tf_op jit(solution)/shard_map/ppermute | solution.py:69
  140.2 2.5 %collective-permute-start.5 = (bf16[256,512]{1,0:T(8,128)(2,1)}, bf16[256,512]{1,0:T(8,128)(2,1)}, u32[]{:S(2)}, u32[]{:S(2)}) collective-permute-start(bf16[256,512]{1,0:T(8,128)(2,1)} %get-tuple-element.98), channel_id=1, source_target_pairs={{0,12},{4,0},{8,4},{12,8},{1,13},{5,1},{9,5},{13,9},{2,14},{6,2},{... | collective-permute-start | bytes 786440 | tf_op jit(solution)/shard_map/ppermute | solution.py:69
  148.9 7.1 %all-to-all-done.5 = bf16[32,32,128]{2,1,0:T(8,128)(2,1)} async-done(((bf16[32,32,128]{2,1,0:T(8,128)(2,1)}), bf16[32,32,128]{2,1,0:T(8,128)(2,1)}, u32[]{:S(2)}, u32[]{:S(2)}) %all-to-all-start.5) | async-done | bytes 262176 | tf_op jit(solution)/shard_map/all_to_all | solution.py:486
  156.0 2.5 %total_cot.1 = (bf16[16,64,128]{2,1,0:T(8,128)(2,1)S(1)}, bf16[16,64,128]{2,1,0:T(8,128)(2,1)S(1)}, bf16[384,128]{1,0:T(8,128)(2,1)S(1)}, f32[2,320]{1,0:T(2,128)S(1)}) custom-call(s32[64]{0:T(128)S(1)} %dynamic-slice_bitcast_fusion.at_ref, bf16[1024,320]{1,0:T(8,128)(2,1)S(1)} %pick.1.p_ref, bf16[1024,128]{1,0:T(8,128)(2,1)} %bitcast.13.r_ref, ...), custom_call_target="tpu_custom_call" | custom-call | flops 170000000 | bytes 2500000 | tf_op jit(solution)/shard_map/total_cot/pallas_call | solution.py:505
  158.5 3.4 %collective-permute-start.6 = (bf16[16,64,128]{2,1,0:T(8,128)(2,1)S(1)}, bf16[16,64,128]{2,1,0:T(8,128)(2,1)S(1)}, u32[]{:S(2)}, u32[]{:S(2)}) collective-permute-start(bf16[16,64,128]{2,1,0:T(8,128)(2,1)S(1)} %get-tuple-element.102), channel_id=1, source_target_pairs={{0,16},{16,0},{1,17},{17,1},{2,18},{18,2},{3,19},{19,3},{4,20},{20... | collective-permute-start | bytes 786440 | tf_op jit(solution)/shard_map/ppermute | solution.py:519
  164.1 17.7 %all_to_all.44.r_ref = bf16[16,72,384]{2,1,0:T(8,128)(2,1)S(1)} all-to-all(bf16[16,72,384]{2,1,0:T(8,128)(2,1)S(1)} %join_cores.1), channel_id=1, replica_groups=mesh['z'=16,'c'=2,'y'=4,'x'=4] {'y','x'}, dimensions={0} | all-to-all | bytes 1769472 | tf_op jit(solution)/shard_map/all_to_all | solution.py:544
  182.6 5.7 %all-to-all-start.7 = ((bf16[16,32,128]{2,1,0:T(8,128)(2,1)}), bf16[16,32,128]{2,1,0:T(8,128)(2,1)S(1)}, u32[]{:S(2)}, u32[]{:S(2)}) async-start(bf16[16,32,128]{2,1,0:T(8,128)(2,1)} %proj_part.1), calls=%async_computation.7 | async-start | bytes 262144 | tf_op jit(solution)/shard_map/all_to_all | solution.py:557
  190.2 4.6 %collective-permute-start.9 = (bf16[192,512]{1,0:T(8,128)(2,1)S(1)}, bf16[192,512]{1,0:T(8,128)(2,1)S(1)}, u32[]{:S(2)}, u32[]{:S(2)}) collective-permute-start(bf16[192,512]{1,0:T(8,128)(2,1)S(1)} %copy-done.18), channel_id=1, source_target_pairs={{0,3},{1,0},{2,1},{3,2},{4,7},{5,4},{6,5},{7,6},{8,11},{9,8},{10,9... | collective-permute-start | bytes 589832 | tf_op jit(solution)/shard_map/ppermute | solution.py:69
  197.0 4.2 %collective-permute-start.10 = (f32[64,128]{1,0:T(8,128)S(1)}, f32[64,128]{1,0:T(8,128)S(1)}, u32[]{:S(2)}, u32[]{:S(2)}) collective-permute-start(f32[64,128]{1,0:T(8,128)S(1)} %get-tuple-element.119), channel_id=1, source_target_pairs={{16,0},{32,16},{48,32},{64,48},{80,64},{96,80},{112,96},{128,112},... | collective-permute-start | bytes 98312 | tf_op jit(solution)/shard_map/ppermute | solution.py:578
  201.3 3.3 %collective-permute-done.10.next_ref = f32[64,128]{1,0:T(8,128)S(1)} collective-permute-done((f32[64,128]{1,0:T(8,128)S(1)}, f32[64,128]{1,0:T(8,128)S(1)}, u32[]{:S(2)}, u32[]{:S(2)}) %collective-permute-start.10) | collective-permute-done | bytes 32800 | tf_op jit(solution)/shard_map/ppermute | solution.py:578
  (83 shorter events, 28.9 us)
Async XLA Ops:
  0.6 21.0 %copy-start.4 = (bf16[1,64,2048]{2,1,0:T(8,128)(2,1)S(1)}, bf16[1,64,2048]{2,1,0:T(8,128)(2,1)}, u32[]{:S(2)}) copy-start(bf16[1,64,2048]{2,1,0:T(8,128)(2,1)} %param.18) | copy-start | bytes 786436
  0.7 21.0 %copy-start.5 = (bf16[1,64,2048]{2,1,0:T(8,128)(2,1)S(1)}, bf16[1,64,2048]{2,1,0:T(8,128)(2,1)}, u32[]{:S(2)}) copy-start(bf16[1,64,2048]{2,1,0:T(8,128)(2,1)} %param.19) | copy-start | bytes 786436
  0.7 21.0 %copy-start.6 = (bf16[1,64,2048]{2,1,0:T(8,128)(2,1)S(1)}, bf16[1,64,2048]{2,1,0:T(8,128)(2,1)}, u32[]{:S(2)}) copy-start(bf16[1,64,2048]{2,1,0:T(8,128)(2,1)} %param.20) | copy-start | bytes 786436
  3.6 50.4 %all-to-all-start = ((bf16[32,32,256]{2,1,0:T(8,128)(2,1)}), bf16[32,32,256]{2,1,0:T(8,128)(2,1)}, u32[]{:S(2)}, u32[]{:S(2)}) async-start(bf16[32,32,256]{2,1,0:T(8,128)(2,1)} %bitcast.35), calls=%async_computation | async-start | bytes 1048576 | tf_op jit(solution)/shard_map/all_to_all | solution.py:433
  22.5 10.7 %collective-permute-start = (bf16[320,512]{1,0:T(8,128)(2,1)S(1)}, bf16[320,512]{1,0:T(8,128)(2,1)S(1)}, u32[]{:S(2)}, u32[]{:S(2)}) collective-permute-start(bf16[320,512]{1,0:T(8,128)(2,1)S(1)} %get-tuple-element.73), channel_id=1, source_target_pairs={{0,1},{1,2},{2,3},{3,0},{4,5},{5,6},{6,7},{7,4},{8,9},{9,10},{10,1... | collective-permute-start | bytes 983048 | tf_op jit(solution)/shard_map/ppermute | solution.py:69
  25.7 10.9 %collective-permute-start.1 = (bf16[320,512]{1,0:T(8,128)(2,1)S(1)}, bf16[320,512]{1,0:T(8,128)(2,1)S(1)}, u32[]{:S(2)}, u32[]{:S(2)}) collective-permute-start(bf16[320,512]{1,0:T(8,128)(2,1)S(1)} %get-tuple-element.74), channel_id=1, source_target_pairs={{0,2},{1,3},{2,0},{3,1},{4,6},{5,7},{6,4},{7,5},{8,10},{9,11},{10,... | collective-permute-start | bytes 983048 | tf_op jit(solution)/shard_map/ppermute | solution.py:69
  30.2 8.2 %collective-permute-start.2 = (bf16[320,512]{1,0:T(8,128)(2,1)S(1)}, bf16[320,512]{1,0:T(8,128)(2,1)S(1)}, u32[]{:S(2)}, u32[]{:S(2)}) collective-permute-start(bf16[320,512]{1,0:T(8,128)(2,1)S(1)} %get-tuple-element.75), channel_id=1, source_target_pairs={{0,3},{1,0},{2,1},{3,2},{4,7},{5,4},{6,5},{7,6},{8,11},{9,8},{10,9... | collective-permute-start | bytes 983048 | tf_op jit(solution)/shard_map/ppermute | solution.py:69
  111.9 30.8 %copy-start.14 = (s32[2,320]{1,0:T(2,128)S(1)}, s32[2,320]{1,0:T(2,128)}, u32[]{:S(2)}) copy-start(s32[2,320]{1,0:T(2,128)} %get-tuple-element.67.t_ref) | copy-start | bytes 7684
  125.2 30.8 %all-to-all-start.5 = ((bf16[32,32,128]{2,1,0:T(8,128)(2,1)}), bf16[32,32,128]{2,1,0:T(8,128)(2,1)}, u32[]{:S(2)}, u32[]{:S(2)}) async-start(bf16[32,32,128]{2,1,0:T(8,128)(2,1)} %bitcast.12), calls=%async_computation.5 | async-start | bytes 524288 | tf_op jit(solution)/shard_map/all_to_all | solution.py:486
  134.3 21.7 %collective-permute-start.3 = (bf16[256,512]{1,0:T(8,128)(2,1)}, bf16[256,512]{1,0:T(8,128)(2,1)S(1)}, u32[]{:S(2)}, u32[]{:S(2)}) collective-permute-start(bf16[256,512]{1,0:T(8,128)(2,1)} %get-tuple-element.96), channel_id=1, source_target_pairs={{0,4},{4,8},{8,12},{12,0},{1,5},{5,9},{9,13},{13,1},{2,6},{6,10},{... | collective-permute-start | bytes 786440 | tf_op jit(solution)/shard_map/ppermute | solution.py:69
  136.5 19.5 %collective-permute-start.4 = (bf16[256,512]{1,0:T(8,128)(2,1)}, bf16[256,512]{1,0:T(8,128)(2,1)}, u32[]{:S(2)}, u32[]{:S(2)}) collective-permute-start(bf16[256,512]{1,0:T(8,128)(2,1)} %get-tuple-element.97), channel_id=1, source_target_pairs={{0,8},{4,12},{8,0},{12,4},{1,9},{5,13},{9,1},{13,5},{2,10},{6,14},... | collective-permute-start | bytes 786440 | tf_op jit(solution)/shard_map/ppermute | solution.py:69
  140.2 15.8 %collective-permute-start.5 = (bf16[256,512]{1,0:T(8,128)(2,1)}, bf16[256,512]{1,0:T(8,128)(2,1)}, u32[]{:S(2)}, u32[]{:S(2)}) collective-permute-start(bf16[256,512]{1,0:T(8,128)(2,1)} %get-tuple-element.98), channel_id=1, source_target_pairs={{0,12},{4,0},{8,4},{12,8},{1,13},{5,1},{9,5},{13,9},{2,14},{6,2},{... | collective-permute-start | bytes 786440 | tf_op jit(solution)/shard_map/ppermute | solution.py:69
  158.5 5.4 %collective-permute-start.6 = (bf16[16,64,128]{2,1,0:T(8,128)(2,1)S(1)}, bf16[16,64,128]{2,1,0:T(8,128)(2,1)S(1)}, u32[]{:S(2)}, u32[]{:S(2)}) collective-permute-start(bf16[16,64,128]{2,1,0:T(8,128)(2,1)S(1)} %get-tuple-element.102), channel_id=1, source_target_pairs={{0,16},{16,0},{1,17},{17,1},{2,18},{18,2},{3,19},{19,3},{4,20},{20... | collective-permute-start | bytes 786440 | tf_op jit(solution)/shard_map/ppermute | solution.py:519
  164.1 24.2 %copy-start.20 = (bf16[192,512]{1,0:T(8,128)(2,1)S(1)}, bf16[192,512]{1,0:T(8,128)(2,1)}, u32[]{:S(2)}) copy-start(bf16[192,512]{1,0:T(8,128)(2,1)} %copy-done.19) | copy-start | bytes 589828
  164.1 26.1 %copy-start.18 = (bf16[192,512]{1,0:T(8,128)(2,1)S(1)}, bf16[192,512]{1,0:T(8,128)(2,1)}, u32[]{:S(2)}) copy-start(bf16[192,512]{1,0:T(8,128)(2,1)} %copy-done.17) | copy-start | bytes 589828
  164.1 30.7 %copy-start.16 = (bf16[192,512]{1,0:T(8,128)(2,1)S(1)}, bf16[192,512]{1,0:T(8,128)(2,1)}, u32[]{:S(2)}) copy-start(bf16[192,512]{1,0:T(8,128)(2,1)} %copy-done.15) | copy-start | bytes 589828
  181.8 22.8 %copy-start.12 = (bf16[320,64]{0,1:T(8,128)(2,1)S(1)}, bf16[320,64]{0,1:T(8,128)(2,1)}, u32[]{:S(2)}) copy-start(bf16[320,64]{0,1:T(8,128)(2,1)} %param.22) | copy-start | bytes 122884
  181.8 22.8 %copy-start.13 = (bf16[320,64]{0,1:T(8,128)(2,1)S(1)}, bf16[320,64]{0,1:T(8,128)(2,1)}, u32[]{:S(2)}) copy-start(bf16[320,64]{0,1:T(8,128)(2,1)} %param.21) | copy-start | bytes 122884
  181.8 24.7 %copy-start.10 = (bf16[192,512]{1,0:T(8,128)(2,1)S(1)}, bf16[192,512]{1,0:T(8,128)(2,1)}, u32[]{:S(2)}) copy-start(bf16[192,512]{1,0:T(8,128)(2,1)} %copy-done.9) | copy-start | bytes 589828
  182.6 25.8 %all-to-all-start.7 = ((bf16[16,32,128]{2,1,0:T(8,128)(2,1)}), bf16[16,32,128]{2,1,0:T(8,128)(2,1)S(1)}, u32[]{:S(2)}, u32[]{:S(2)}) async-start(bf16[16,32,128]{2,1,0:T(8,128)(2,1)} %proj_part.1), calls=%async_computation.7 | async-start | bytes 262144 | tf_op jit(solution)/shard_map/all_to_all | solution.py:557
  188.3 18.2 %collective-permute-start.7 = (bf16[192,512]{1,0:T(8,128)(2,1)S(1)}, bf16[192,512]{1,0:T(8,128)(2,1)S(1)}, u32[]{:S(2)}, u32[]{:S(2)}) collective-permute-start(bf16[192,512]{1,0:T(8,128)(2,1)S(1)} %copy-done.20), channel_id=1, source_target_pairs={{0,1},{1,2},{2,3},{3,0},{4,5},{5,6},{6,7},{7,4},{8,9},{9,10},{10,1... | collective-permute-start | bytes 589832 | tf_op jit(solution)/shard_map/ppermute | solution.py:69
  190.2 16.3 %collective-permute-start.9 = (bf16[192,512]{1,0:T(8,128)(2,1)S(1)}, bf16[192,512]{1,0:T(8,128)(2,1)S(1)}, u32[]{:S(2)}, u32[]{:S(2)}) collective-permute-start(bf16[192,512]{1,0:T(8,128)(2,1)S(1)} %copy-done.18), channel_id=1, source_target_pairs={{0,3},{1,0},{2,1},{3,2},{4,7},{5,4},{6,5},{7,6},{8,11},{9,8},{10,9... | collective-permute-start | bytes 589832 | tf_op jit(solution)/shard_map/ppermute | solution.py:69
  194.8 11.7 %collective-permute-start.8 = (bf16[192,512]{1,0:T(8,128)(2,1)S(1)}, bf16[192,512]{1,0:T(8,128)(2,1)S(1)}, u32[]{:S(2)}, u32[]{:S(2)}) collective-permute-start(bf16[192,512]{1,0:T(8,128)(2,1)S(1)} %copy-done.16), channel_id=1, source_target_pairs={{0,2},{1,3},{2,0},{3,1},{4,6},{5,7},{6,4},{7,5},{8,10},{9,11},{10,... | collective-permute-start | bytes 589832 | tf_op jit(solution)/shard_map/ppermute | solution.py:69
  197.0 7.6 %collective-permute-start.10 = (f32[64,128]{1,0:T(8,128)S(1)}, f32[64,128]{1,0:T(8,128)S(1)}, u32[]{:S(2)}, u32[]{:S(2)}) collective-permute-start(f32[64,128]{1,0:T(8,128)S(1)} %get-tuple-element.119), channel_id=1, source_target_pairs={{16,0},{32,16},{48,32},{64,48},{80,64},{96,80},{112,96},{128,112},... | collective-permute-start | bytes 98312 | tf_op jit(solution)/shard_map/ppermute | solution.py:578
  (13 other events, 110.5 us)
